TPU v7x, 32 devices: a whole 2x2x4 slice. The times are simulated.
32 devices in a mesh: ep: 32 (over z, y, x, core).
Axes of the slice: x: 2, y: 2, z: 4, core: 2. Of those that a mesh axis runs over, the one named last changes fastest.
Arguments:
- tokens: bfloat16 [256, 2048], P('ep'), may hold values from -6 to 6
- premix_gain: float32 [2048], replicated, may hold values from 0.1 to 1.9
- postmix_gain: float32 [2048], replicated, may hold values from 0.1 to 1.9
- prefeed_gain: float32 [2048], replicated, may hold values from 0.1 to 1.9
- postfeed_gain: float32 [2048], replicated, may hold values from 0.1 to 1.9
- query_weight: bfloat16 [2048, 1024], P('ep'), may hold values from -0.125 to 0.125
- key_weight: bfloat16 [2048, 1024], P('ep'), may hold values from -0.125 to 0.125
- value_weight: bfloat16 [2048, 1024], P('ep'), may hold values from -0.125 to 0.125
- outgate_weight: bfloat16 [2048, 1024], P('ep'), may hold values from -0.125 to 0.125
- ingate_weight: bfloat16 [2048, 8], replicated, may hold values from -0.125 to 0.125
- forget_weight: bfloat16 [2048, 8], replicated, may hold values from -0.125 to 0.125
- ingate_bias: float32 [8], replicated, may hold values from -1 to 1
- forget_bias: float32 [8], replicated, may hold values from -1 to 5
- memory_state: float32 [256, 8, 128, 128], P('ep'), may hold values from -1.25 to 1.25
- normalizer: float32 [256, 8, 128], P('ep'), may hold values from -1.75 to 1.75
- stabilizer: float32 [256, 8], P('ep'), may hold values from -2 to 2
- output_weight: bfloat16 [1024, 2048], P(None, 'ep'), may hold values from -0.1875 to 0.1875
- expert_ids: int32 [256, 6], P('ep'), may hold values from 0 to 31, all different within a row; in each aligned block of 8 rows (0 to 7, 8 to 15, ...) at most 4 rows name the same one
- route_weights: float32 [256, 6], P('ep'), may hold values from 0.2 to 0.8
- expert_gate: bfloat16 [32, 2048, 512], P('ep'), may hold values from -0.125 to 0.125
- expert_up: bfloat16 [32, 2048, 512], P('ep'), may hold values from -0.125 to 0.125
- expert_down: bfloat16 [32, 512, 2048], P('ep'), may hold values from -0.25 to 0.25
- shared_gate: bfloat16 [2048, 512], replicated, may hold values from -0.125 to 0.125
- shared_up: bfloat16 [2048, 512], replicated, may hold values from -0.125 to 0.125
- shared_down: bfloat16 [512, 2048], replicated, may hold values from -0.25 to 0.25
Outputs:
- next_tokens: bfloat16 [256, 2048], P('ep')
- next_memory: float32 [256, 8, 128, 128], P('ep')
- next_normalizer: float32 [256, 8, 128], P('ep')
- next_stabilizer: float32 [256, 8], P('ep')
Inputs may be any that keep to these rules, and one draw needn't show every extreme that they name: `expert_ids`: each row names 6 different experts. Among the rows of one device no expert is named more than 4 times, and in every draw some expert is named exactly 4 times by the rows of some device.
All inputs are finite; a program needn't handle non-finite values.
Results may differ from a plain program's by a relative error of at most 0.0097.
Values may be sent and summed in bfloat16 or wider, within the bound.
A program may use at most 128 MiB of HBM per device.

v0:
```python
import functools

import jax
import jax.numpy as jnp
from jax import lax
from jax.experimental import pallas as pl
from jax.experimental.pallas import tpu as pltpu
from jax.sharding import PartitionSpec as P

epsilon = 1e-06
LANES = 128
GROUPS = 4
MESH = pl.DeviceIdType.MESH
VM = pl.BlockSpec(memory_space=pltpu.VMEM)
ANY = pl.BlockSpec(memory_space=pl.ANY)


def rms_scale(values, gain_row):
    return (
        values * lax.rsqrt(jnp.mean(values * values, axis=-1, keepdims=True) + epsilon) * gain_row
    )


def greet(n, me):
    sem = pltpu.get_barrier_semaphore()

    def signal(i, carry):
        pl.semaphore_signal(
            sem, inc=1, device_id=(lax.rem(me + i, n),), device_id_type=MESH
        )
        return carry

    lax.fori_loop(1, n, signal, 0)


def greeted(n):
    pl.semaphore_wait(pltpu.get_barrier_semaphore(), n - 1)


def send(src, dst, send_sem, recv_sem, peer):
    pltpu.make_async_remote_copy(
        src_ref=src,
        dst_ref=dst,
        send_sem=send_sem,
        recv_sem=recv_sem,
        device_id=(peer,),
        device_id_type=MESH,
    ).start()


def drain(ref, sem):
    pltpu.make_async_copy(ref, ref, sem).wait()


def routing(ids, route_weights, slot_count, capacity):
    sequences, choices = ids.shape
    slot = lax.broadcasted_iota(jnp.int32, (sequences, slot_count), 1).astype(jnp.float32)
    owner = jnp.floor((slot + 0.5) * (1.0 / capacity))
    turn = slot - owner * capacity
    chosen = jnp.zeros((sequences, slot_count), jnp.float32)
    weight_of = jnp.zeros((sequences, slot_count), jnp.float32)
    float_ids = ids.astype(jnp.float32)
    for choice in range(choices):
        same = float_ids[:, choice : choice + 1] == owner
        chosen = jnp.where(same, 1.0, chosen)
        weight_of = jnp.where(same, route_weights[:, choice : choice + 1], weight_of)
    earlier = jnp.zeros((sequences, slot_count), jnp.float32)
    row = lax.broadcasted_iota(jnp.int32, (sequences, slot_count), 0)
    for other in range(sequences - 1):
        earlier = earlier + jnp.where(row > other, chosen[other : other + 1], 0.0)
    slots = jnp.where(earlier == turn, chosen, 0.0)
    return slots, slots * weight_of


def across(left, right):
    return lax.dot_general(
        left, right, (((1,), (1,)), ((), ())), preferred_element_type=jnp.float32
    )


def two_layer(rows, gate_weight, up_weight, down_weight):
    gate_values = jnp.dot(rows, gate_weight, preferred_element_type=jnp.float32)
    up_values = jnp.dot(rows, up_weight, preferred_element_type=jnp.float32)
    inner_rows = (gate_values * jax.nn.sigmoid(gate_values) * up_values).astype(jnp.bfloat16)
    return jnp.dot(inner_rows, down_weight, preferred_element_type=jnp.float32)


def layer_kernel(n, groups, *refs):
    (
        tokens_ref,
        premix_ref,
        postmix_ref,
        prefeed_ref,
        postfeed_ref,
        input_bias_ref,
        forget_bias_ref,
        normalizer_ref,
        stabilizer_ref,
        ids_ref,
        route_ref,
        mix_ref,
        query_ref,
        key_ref,
        value_ref,
        gate_ref,
    ) = refs[:16]
    loads_from = refs[16:25]
    out_ref, projected_ref, gates_ref = refs[25:28]
    loaded = refs[28:37]
    (
        normed_buf,
        rows_buf,
        weight_buf,
        product_buf,
        result_buf,
        mix_buf,
        split_buf,
        gated_src,
        gated_buf,
        columns_buf,
        mixed_buf,
        outgoing,
        arrived,
        answer,
        returned,
        load_sems,
        send_sems,
        recv_sems,
    ) = refs[37:]
    weights = loaded[:6]
    input_weight, forget_weight, memory = loaded[6:]
    me = lax.axis_index("ep")
    members = n // groups
    plane, place = me // members, lax.rem(me, members)
    part_width = rows_buf.shape[2]
    columns = weight_buf.shape[2]
    per_matrix = query_ref.shape[1] // columns
    greet(n, me)
    projections = (query_ref, key_ref, value_ref, gate_ref)

    def column(block):
        return pl.ds(pl.multiple_of(lax.rem(block, per_matrix) * columns, LANES), columns)

    for index, ref in enumerate(projections):

        @pl.when(place // per_matrix == index)
        def _():
            pltpu.make_async_copy(
                ref.at[:, column(place)], weight_buf.at[place], recv_sems.at[1]
            ).start()

    pltpu.make_async_copy(mix_ref, mix_buf.at[place], recv_sems.at[3]).start()
    loads = [
        pltpu.make_async_copy(source, target, load_sems.at[index])
        for index, (source, target) in enumerate(zip(loads_from, loaded))
    ]
    residual = tokens_ref[...].astype(jnp.float32)
    normed = rms_scale(residual, premix_ref[...]).astype(jnp.bfloat16)
    for group in range(groups):
        normed_buf[group] = normed[:, group * part_width : (group + 1) * part_width]
    pltpu.make_async_copy(normed_buf.at[plane], rows_buf.at[me], recv_sems.at[0]).start()
    greeted(n)

    def send_rows(i, carry):
        peer = lax.rem(me + i, n)
        send(
            normed_buf.at[peer // members],
            rows_buf.at[me],
            send_sems.at[0],
            recv_sems.at[0],
            peer,
        )
        return carry

    def send_weights(i, carry):
        block = lax.rem(place + i, members)
        for index, ref in enumerate(projections):

            @pl.when(block // per_matrix == index)
            def _():
                send(
                    ref.at[:, column(block)],
                    weight_buf.at[place],
                    send_sems.at[1],
                    recv_sems.at[1],
                    plane * members + block,
                )

        return carry

    lax.fori_loop(1, members, send_weights, 0)
    lax.fori_loop(1, n, send_rows, 0)
    for index in (6, 7, 8, 3, 4, 5, 0, 1, 2):
        loads[index].start()

    loads[6].wait()
    loads[7].wait()
    input_pre = (
        across(normed, input_weight[...])
        + input_bias_ref[...]
    )
    forget_pre = (
        across(normed, forget_weight[...])
        + forget_bias_ref[...]
    )
    carried = (
        jnp.minimum(forget_pre, 0.0)
        - jnp.log1p(jnp.exp(-jnp.abs(forget_pre)))
        + stabilizer_ref[...]
    )
    next_stabilizer = jnp.maximum(carried, input_pre)
    keep_old = jnp.exp(carried - next_stabilizer)
    write_new = jnp.exp(input_pre - next_stabilizer)
    gates_ref[0] = keep_old
    gates_ref[1] = write_new
    gates_ref[2] = next_stabilizer
    local, capacity, width = outgoing.shape[1:]
    slots, combine = routing(ids_ref[...], route_ref[...], n * local * capacity, capacity)
    dispatch = slots.T.astype(jnp.bfloat16)
    sequences, heads, head_width = memory.shape[:3]
    loads[8].wait()

    def split(s, carry):
        for head in range(heads):
            value = memory[s, head]
            high = value.astype(jnp.bfloat16)
            rows = pl.ds(pl.multiple_of(s * head_width, LANES), head_width)
            split_buf[head, rows, :head_width] = high
            split_buf[head, rows, head_width:] = (value - high.astype(jnp.float32)).astype(
                jnp.bfloat16
            )
        return carry

    lax.fori_loop(0, sequences, split, 0)

    drain(rows_buf, recv_sems.at[0])
    drain(weight_buf, recv_sems.at[1])
    rows = rows_buf[...].reshape(rows_buf.shape[0] * rows_buf.shape[1], part_width)
    weight = weight_buf[...].reshape(weight_buf.shape[0] * weight_buf.shape[1], columns)
    product = jnp.dot(rows, weight, preferred_element_type=jnp.float32)
    product_buf[...] = product.reshape(product_buf.shape).astype(jnp.bfloat16)
    pltpu.make_async_copy(product_buf.at[me], result_buf.at[me], recv_sems.at[2]).start()

    def exchange(source, target, stage):
        def one(i, carry):
            peer = lax.rem(me + i, n)
            send(source.at[peer], target.at[me], send_sems.at[stage], recv_sems.at[stage], peer)
            return carry

        lax.fori_loop(1, n, one, 0)

    def send_mix(i, carry):
        send(
            mix_ref,
            mix_buf.at[place],
            send_sems.at[3],
            recv_sems.at[3],
            plane * members + lax.rem(place + i, members),
        )
        return carry

    def line(source, target, stage):
        for i in range(1, groups):
            peer = lax.rem(plane + i, groups)
            send(
                source(peer),
                target.at[plane],
                send_sems.at[stage],
                recv_sems.at[stage],
                peer * members + place,
            )

    exchange(product_buf, result_buf, 2)
    lax.fori_loop(1, members, send_mix, 0)
    drain(result_buf, recv_sems.at[2])
    for member in range(members):
        total = result_buf[member].astype(jnp.float32)
        for group in range(1, groups):
            total = total + result_buf[group * members + member].astype(jnp.float32)
        total = total.astype(jnp.bfloat16).astype(jnp.float32)
        projected_ref[:, member * columns : (member + 1) * columns] = total
    memory_width = heads * head_width
    row = lax.broadcasted_iota(jnp.int32, (sequences, head_width), 0)
    for head in range(heads):

        def piece(matrix):
            start = matrix * memory_width + head * head_width
            return projected_ref[:, start : start + head_width]

        span = slice(head * head_width, (head + 1) * head_width)
        query, value, out_gate = piece(0), piece(2), piece(3)
        key = piece(1) * head_width ** (-0.5)
        keep, write = keep_old[:, head : head + 1], write_new[:, head : head + 1]
        local_score = write * jnp.sum(query * key, axis=-1, keepdims=True)
        denominator = (
            keep * jnp.sum(normalizer_ref[:, head, :] * query, axis=-1, keepdims=True) + local_score
        )
        narrow = query.astype(jnp.bfloat16)
        reads = lax.dot_general(
            jnp.concatenate([narrow, narrow], axis=1),
            split_buf[head],
            (((1,), (1,)), ((), ())),
            preferred_element_type=jnp.float32,
        )
        read = jnp.zeros((sequences, head_width), jnp.float32)
        for s in range(sequences):
            read = jnp.where(row == s, reads[:, s * head_width : (s + 1) * head_width], read)
        memory_read = (keep * read + local_score * value) / jnp.maximum(
            jnp.abs(denominator), 1.0
        )
        gated_src[:, span] = (jax.nn.sigmoid(out_gate) * memory_read).astype(jnp.bfloat16)

    pltpu.make_async_copy(gated_src, gated_buf.at[plane], recv_sems.at[4]).start()
    line(lambda peer: gated_src, gated_buf, 4)
    drain(mix_buf, recv_sems.at[3])
    drain(gated_buf, recv_sems.at[4])
    gated = gated_buf[...].reshape(gated_buf.shape[0] * gated_buf.shape[1], gated_buf.shape[2])
    mix_weight = mix_buf[...].reshape(mix_buf.shape[0] * mix_buf.shape[1], mix_buf.shape[2])
    columns_buf[...] = (
        lax.dot_general(
            gated, mix_weight, (((1,), (1,)), ((), ())), preferred_element_type=jnp.float32
        )
        .reshape(columns_buf.shape)
        .astype(jnp.bfloat16)
    )
    pltpu.make_async_copy(columns_buf.at[plane], mixed_buf.at[plane], recv_sems.at[5]).start()
    line(lambda peer: columns_buf.at[peer], mixed_buf, 5)
    drain(mixed_buf, recv_sems.at[5])
    mixed = jnp.concatenate([mixed_buf[group] for group in range(groups)], axis=1)
    after_mix = (residual + rms_scale(mixed.astype(jnp.float32), postmix_ref[...])).astype(
        jnp.bfloat16
    )
    after_float = after_mix.astype(jnp.float32)
    token_rows = rms_scale(after_float, prefeed_ref[...]).astype(jnp.bfloat16)
    outgoing[...] = (
        jnp.dot(dispatch, token_rows, preferred_element_type=jnp.float32)
        .reshape(outgoing.shape)
        .astype(jnp.bfloat16)
    )
    pltpu.make_async_copy(outgoing.at[me], arrived.at[me], recv_sems.at[6]).start()
    exchange(outgoing, arrived, 6)
    for index in (3, 4, 5):
        loads[index].wait()
    shared_out = two_layer(token_rows, weights[3][...], weights[4][...], weights[5][...])
    for index in (0, 1, 2):
        loads[index].wait()
    drain(arrived, recv_sems.at[6])
    for item in range(local):
        block = arrived[:, item].astype(jnp.float32).reshape(n * capacity, width)
        answer[:, item] = (
            two_layer(
                block.astype(jnp.bfloat16),
                weights[0][item],
                weights[1][item],
                weights[2][item],
            )
            .reshape(n, capacity, width)
            .astype(jnp.bfloat16)
        )
    pltpu.make_async_copy(answer.at[me], returned.at[me], recv_sems.at[7]).start()
    exchange(answer, returned, 7)
    high = combine.astype(jnp.bfloat16)
    low = (combine - high.astype(jnp.float32)).astype(jnp.bfloat16)
    drain(returned, recv_sems.at[7])
    picked = (
        returned[...].astype(jnp.float32).reshape(combine.shape[1], width).astype(jnp.bfloat16)
    )
    combined = (
        shared_out
        + jnp.dot(high, picked, preferred_element_type=jnp.float32)
        + jnp.dot(low, picked, preferred_element_type=jnp.float32)
    )
    out_ref[...] = (after_float + rms_scale(combined, postfeed_ref[...])).astype(jnp.bfloat16)
    drain(rows_buf.at[pl.ds(0, n - 1)], send_sems.at[0])
    drain(weight_buf.at[pl.ds(0, members - 1)], send_sems.at[1])
    drain(result_buf.at[pl.ds(0, n - 1)], send_sems.at[2])
    drain(mix_buf.at[pl.ds(0, members - 1)], send_sems.at[3])
    drain(gated_buf.at[pl.ds(0, groups - 1)], send_sems.at[4])
    drain(mixed_buf.at[pl.ds(0, groups - 1)], send_sems.at[5])
    drain(arrived.at[pl.ds(0, n - 1)], send_sems.at[6])
    drain(returned.at[pl.ds(0, n - 1)], send_sems.at[7])


def layer(n, groups, small, projections, loads, capacity):
    tokens, mix_weight = small[0], small[-1]
    sequences, width = tokens.shape
    depth, columns = projections[0].shape
    members = n // groups
    wide = 4 * columns // members
    local = loads[0].shape[0]
    heads, head_width = loads[8].shape[1:3]
    narrow = functools.partial(pltpu.VMEM, dtype=jnp.bfloat16)
    slots = narrow((n, local, capacity, width))
    pieces = narrow((groups, sequences, width // groups))
    return pl.pallas_call(
        functools.partial(layer_kernel, n, groups),
        out_shape=(
            jax.ShapeDtypeStruct((sequences, width), jnp.bfloat16),
            jax.ShapeDtypeStruct((sequences, 4 * columns), jnp.float32),
            jax.ShapeDtypeStruct((3, sequences, heads), jnp.float32),
        ),
        in_specs=[VM] * len(small) + [ANY] * (len(projections) + len(loads)),
        out_specs=(VM, VM, VM),
        scratch_shapes=[pltpu.VMEM(w.shape, w.dtype) for w in loads]
        + [
            pieces,
            narrow((n, sequences, width // groups)),
            narrow((members, depth, wide)),
            narrow((n, sequences, wide)),
            narrow((n, sequences, wide)),
            narrow((members,) + mix_weight.shape),
            narrow((heads, sequences * head_width, 2 * head_width)),
            narrow((sequences, columns)),
            narrow((groups, sequences, columns)),
            pieces,
            pieces,
        ]
        + [slots] * 4
        + [
            pltpu.SemaphoreType.DMA((len(loads),)),
            pltpu.SemaphoreType.DMA((8,)),
            pltpu.SemaphoreType.DMA((8,)),
        ],
        compiler_params=pltpu.CompilerParams(
            collective_id=0, has_side_effects=True, vmem_limit_bytes=56 * 1024 * 1024
        ),
    )(*small, *projections, *loads)


def state_kernel(
    tokens_ref,
    projected_ref,
    gates_ref,
    normalizer_ref,
    memory_ref,
    next_tokens_ref,
    next_memory_ref,
    next_normalizer_ref,
    next_stabilizer_ref,
):
    step = pl.program_id(0)
    block, heads, head_width = memory_ref.shape[:3]
    memory_width = heads * head_width
    scale = head_width ** (-0.5)

    @pl.when(step == 0)
    def _():
        next_tokens_ref[...] = tokens_ref[...]
        next_stabilizer_ref[...] = gates_ref[2]
        keep_all, write_all = gates_ref[0], gates_ref[1]
        for head in range(heads):
            start = memory_width + head * head_width
            next_normalizer_ref[:, head, :] = keep_all[:, head : head + 1] * normalizer_ref[
                :, head, :
            ] + write_all[:, head : head + 1] * (
                projected_ref[:, start : start + head_width] * scale
            )

    for item in range(block):
        row = pl.ds(step * block + item, 1)
        keep, write = gates_ref[0, row, :], gates_ref[1, row, :]
        keys = projected_ref[row, memory_width : 2 * memory_width] * scale
        values = projected_ref[row, 2 * memory_width : 3 * memory_width]
        stacked = jnp.concatenate(
            [
                write[:, head : head + 1] * values[:, head * head_width : (head + 1) * head_width]
                for head in range(heads)
            ],
            axis=0,
        ).T
        for head in range(heads):
            next_memory_ref[item, head] = (
                keep[:, head : head + 1] * memory_ref[item, head]
                + stacked[:, head : head + 1]
                * keys[:, head * head_width : (head + 1) * head_width]
            )


def write_state(tokens, projected, gates, normalizer, memory):
    sequences = memory.shape[0]
    steps = 4
    block = (sequences // steps,) + memory.shape[1:]

    def whole(array):
        return pl.BlockSpec(array.shape, lambda i, rank=array.ndim: (0,) * rank)

    moving = pl.BlockSpec(block, lambda i: (i, 0, 0, 0))
    stabilizer = jax.ShapeDtypeStruct(gates.shape[1:], jnp.float32)
    return pl.pallas_call(
        state_kernel,
        grid=(steps,),
        out_shape=(
            jax.ShapeDtypeStruct(tokens.shape, tokens.dtype),
            jax.ShapeDtypeStruct(memory.shape, memory.dtype),
            jax.ShapeDtypeStruct(normalizer.shape, normalizer.dtype),
            stabilizer,
        ),
        in_specs=[whole(tokens), whole(projected), whole(gates), whole(normalizer), moving],
        out_specs=(whole(tokens), moving, whole(normalizer), whole(stabilizer)),
        compiler_params=pltpu.CompilerParams(dimension_semantics=("arbitrary",)),
    )(tokens, projected, gates, normalizer, memory)


def on_device(
    tokens,
    premix_gain,
    postmix_gain,
    prefeed_gain,
    postfeed_gain,
    query_weight,
    key_weight,
    value_weight,
    outgate_weight,
    ingate_weight,
    forget_weight,
    ingate_bias,
    forget_bias,
    memory_state,
    normalizer,
    stabilizer,
    output_weight,
    expert_ids,
    route_weights,
    expert_gate,
    expert_up,
    expert_down,
    shared_gate,
    shared_up,
    shared_down,
):
    sequences = tokens.shape[0]
    devices = lax.axis_size("ep")
    experts_total = expert_gate.shape[0] * devices
    choose_count = expert_ids.shape[1]
    capacity = min(
        sequences, max(2, 2 * ((sequences * choose_count + experts_total - 1) // experts_total))
    )
    next_tokens, projected, gates = layer(
        devices,
        GROUPS,
        (
            tokens,
            premix_gain[None],
            postmix_gain[None],
            prefeed_gain[None],
            postfeed_gain[None],
            ingate_bias[None],
            forget_bias[None],
            normalizer,
            stabilizer,
            expert_ids,
            route_weights,
            output_weight.T,
        ),
        (query_weight, key_weight, value_weight, outgate_weight),
        (
            expert_gate,
            expert_up,
            expert_down,
            shared_gate,
            shared_up,
            shared_down,
            ingate_weight.T,
            forget_weight.T,
            memory_state,
        ),
        capacity,
    )
    return write_state(next_tokens, projected, gates, normalizer, memory_state)


def solution(mesh):
    in_specs = (
        P("ep", None),
        P(),
        P(),
        P(),
        P(),
        P("ep", None),
        P("ep", None),
        P("ep", None),
        P("ep", None),
        P(),
        P(),
        P(),
        P(),
        P("ep", None, None, None),
        P("ep", None, None),
        P("ep", None),
        P(None, "ep"),
        P("ep", None),
        P("ep", None),
        P("ep", None, None),
        P("ep", None, None),
        P("ep", None, None),
        P(),
        P(),
        P(),
    )
    out_specs = (P("ep", None), P("ep", None, None, None), P("ep", None, None), P("ep", None))
    return jax.shard_map(
        on_device, mesh=mesh, in_specs=in_specs, out_specs=out_specs, check_vma=False
    )
```

profile of v0, /device:TPU:29, one launch (start us, length us, event | category | flops | bytes accessed | tf_op | source)
XLA Modules:
  0.0 71.8 jit_solution(10846911405873004690)
XLA Ops:
  0.6 64.5 %shard_map.264 = (bf16[8,2048]{1,0:T(8,128)(2,1)}, f32[8,4096]{1,0:T(8,128)}, f32[3,8,8]{2,1,0:T(8,128)}) custom-call(bf16[8,2048]{1,0:T(8,128)(2,1)} %refs_0_.1, f32[1,2048]{1,0:T(1,128)} %bitcast.12, f32[1,2048]{1,0:T(1,128)} %bitcast.13, f32[1,2048]{1,0:T(1,128)} %bitcast.14, f32[1,2048]{1,0:T(1,128)} %bitcast.15, f32[1,8]{1,0:T(1,128)} %bitcast.16, ...), custom_call_target="tpu_custom_call" | custom-call | tf_op jit(solution)/shard_map/pallas_call | solution.py:395
  65.2 6.7 %shard_map.265 = (bf16[8,2048]{1,0:T(8,128)(2,1)}, f32[8,8,128,128]{3,2,1,0:T(8,128)}, f32[8,8,128]{2,1,0:T(8,128)}, f32[8,8]{1,0:T(8,128)}) custom-call(bf16[8,2048]{1,0:T(8,128)(2,1)} %get-tuple-element.7.tokens_ref, f32[8,4096]{1,0:T(8,128)} %get-tuple-element.8.projected_ref, f32[3,8,8]{2,1,0:T(8,128)} %get-tuple-element.9.gates_ref, ...), custom_call_target="tpu_custom_call" | custom-call | tf_op jit(solution)/shard_map/pallas_call | solution.py:489
where the time goes:
time: 72.1 us; the launch traced here: 71.8 us
  Pallas kernels  71.2 us (99%)
    pallas_call x1, Pallas kernels, layer(): pl.pallas_call(functools.partial(layer_kernel, n, groups), out_shape=(jax...  64.5 us
    pallas_call x1, Pallas kernels, write_state(): pl.pallas_call(state_kernel, grid=(steps,), out_shape=(jax.ShapeDtypeStru...  6.65 us

commit v1 on v0

--- a/solution.py
+++ b/solution.py
@@ -105,8 +105,8 @@
         gate_ref,
     ) = refs[:16]
     loads_from = refs[16:25]
-    out_ref, projected_ref, gates_ref = refs[25:28]
-    loaded = refs[28:37]
+    out_ref, next_memory_ref, next_normalizer_ref, next_stabilizer_ref = refs[25:29]
+    loaded = refs[29:38]
     (
         normed_buf,
         rows_buf,
@@ -123,16 +123,21 @@
         arrived,
         answer,
         returned,
+        projected_ref,
+        gates_ref,
         load_sems,
         send_sems,
         recv_sems,
-    ) = refs[37:]
+    ) = refs[38:]
     weights = loaded[:6]
     input_weight, forget_weight, memory = loaded[6:]
     me = lax.axis_index("ep")
     members = n // groups
     plane, place = me // members, lax.rem(me, members)
-    part_width = rows_buf.shape[2]
+    chips, near_chips = n // 2, members // 2
+    chip, core, near_chip = me // 2, lax.rem(me, 2), place // 2
+    partner = me + 1 - 2 * core
+    part_width = rows_buf.shape[3]
     columns = weight_buf.shape[2]
     per_matrix = query_ref.shape[1] // columns
     greet(n, me)
@@ -149,7 +154,7 @@
                 ref.at[:, column(place)], weight_buf.at[place], recv_sems.at[1]
             ).start()
 
-    pltpu.make_async_copy(mix_ref, mix_buf.at[place], recv_sems.at[3]).start()
+    pltpu.make_async_copy(mix_ref, mix_buf.at[near_chip, core], recv_sems.at[3]).start()
     loads = [
         pltpu.make_async_copy(source, target, load_sems.at[index])
         for index, (source, target) in enumerate(zip(loads_from, loaded))
@@ -158,14 +163,16 @@
     normed = rms_scale(residual, premix_ref[...]).astype(jnp.bfloat16)
     for group in range(groups):
         normed_buf[group] = normed[:, group * part_width : (group + 1) * part_width]
-    pltpu.make_async_copy(normed_buf.at[plane], rows_buf.at[me], recv_sems.at[0]).start()
+    pltpu.make_async_copy(
+        normed_buf.at[plane], rows_buf.at[chip, core], recv_sems.at[0]
+    ).start()
     greeted(n)
 
     def send_rows(i, carry):
-        peer = lax.rem(me + i, n)
+        peer = lax.rem(me + 2 * i, n)
         send(
             normed_buf.at[peer // members],
-            rows_buf.at[me],
+            rows_buf.at[chip, core],
             send_sems.at[0],
             recv_sems.at[0],
             peer,
@@ -188,8 +195,8 @@
 
         return carry
 
+    lax.fori_loop(1, chips, send_rows, 0)
     lax.fori_loop(1, members, send_weights, 0)
-    lax.fori_loop(1, n, send_rows, 0)
     for index in (6, 7, 8, 3, 4, 5, 0, 1, 2):
         loads[index].start()
 
@@ -213,7 +220,7 @@
     write_new = jnp.exp(input_pre - next_stabilizer)
     gates_ref[0] = keep_old
     gates_ref[1] = write_new
-    gates_ref[2] = next_stabilizer
+    next_stabilizer_ref[...] = next_stabilizer
     local, capacity, width = outgoing.shape[1:]
     slots, combine = routing(ids_ref[...], route_ref[...], n * local * capacity, capacity)
     dispatch = slots.T.astype(jnp.bfloat16)
@@ -233,9 +240,13 @@
 
     lax.fori_loop(0, sequences, split, 0)
 
-    drain(rows_buf, recv_sems.at[0])
+    drain(rows_buf.at[:, core], recv_sems.at[0])
+    send(
+        rows_buf.at[:, core], rows_buf.at[:, core], send_sems.at[8], recv_sems.at[8], partner
+    )
     drain(weight_buf, recv_sems.at[1])
-    rows = rows_buf[...].reshape(rows_buf.shape[0] * rows_buf.shape[1], part_width)
+    drain(rows_buf.at[:, 1 - core], recv_sems.at[8])
+    rows = rows_buf[...].reshape(n * rows_buf.shape[2], part_width)
     weight = weight_buf[...].reshape(weight_buf.shape[0] * weight_buf.shape[1], columns)
     product = jnp.dot(rows, weight, preferred_element_type=jnp.float32)
     product_buf[...] = product.reshape(product_buf.shape).astype(jnp.bfloat16)
@@ -252,10 +263,10 @@
     def send_mix(i, carry):
         send(
             mix_ref,
-            mix_buf.at[place],
+            mix_buf.at[near_chip, core],
             send_sems.at[3],
             recv_sems.at[3],
-            plane * members + lax.rem(place + i, members),
+            plane * members + lax.rem(place + 2 * i, members),
         )
         return carry
 
@@ -271,7 +282,7 @@
             )
 
     exchange(product_buf, result_buf, 2)
-    lax.fori_loop(1, members, send_mix, 0)
+    lax.fori_loop(1, near_chips, send_mix, 0)
     drain(result_buf, recv_sems.at[2])
     for member in range(members):
         total = result_buf[member].astype(jnp.float32)
@@ -312,10 +323,12 @@
 
     pltpu.make_async_copy(gated_src, gated_buf.at[plane], recv_sems.at[4]).start()
     line(lambda peer: gated_src, gated_buf, 4)
-    drain(mix_buf, recv_sems.at[3])
+    drain(mix_buf.at[:, core], recv_sems.at[3])
+    send(mix_buf.at[:, core], mix_buf.at[:, core], send_sems.at[9], recv_sems.at[9], partner)
     drain(gated_buf, recv_sems.at[4])
+    drain(mix_buf.at[:, 1 - core], recv_sems.at[9])
     gated = gated_buf[...].reshape(gated_buf.shape[0] * gated_buf.shape[1], gated_buf.shape[2])
-    mix_weight = mix_buf[...].reshape(mix_buf.shape[0] * mix_buf.shape[1], mix_buf.shape[2])
+    mix_weight = mix_buf[...].reshape(members * mix_buf.shape[2], mix_buf.shape[3])
     columns_buf[...] = (
         lax.dot_general(
             gated, mix_weight, (((1,), (1,)), ((), ())), preferred_element_type=jnp.float32
@@ -339,6 +352,36 @@
     )
     pltpu.make_async_copy(outgoing.at[me], arrived.at[me], recv_sems.at[6]).start()
     exchange(outgoing, arrived, 6)
+    key_scale = head_width ** (-0.5)
+    for head in range(heads):
+        start = memory_width + head * head_width
+        next_normalizer_ref[:, head, :] = keep_old[:, head : head + 1] * normalizer_ref[
+            :, head, :
+        ] + write_new[:, head : head + 1] * (
+            projected_ref[:, start : start + head_width] * key_scale
+        )
+
+    def update(s, carry):
+        line_of = pl.ds(s, 1)
+        keep, write = gates_ref[0, line_of, :], gates_ref[1, line_of, :]
+        keys = projected_ref[line_of, memory_width : 2 * memory_width] * key_scale
+        values = projected_ref[line_of, 2 * memory_width : 3 * memory_width]
+        stacked = jnp.concatenate(
+            [
+                write[:, head : head + 1] * values[:, head * head_width : (head + 1) * head_width]
+                for head in range(heads)
+            ],
+            axis=0,
+        ).T
+        for head in range(heads):
+            next_memory_ref[s, head] = (
+                keep[:, head : head + 1] * memory[s, head]
+                + stacked[:, head : head + 1]
+                * keys[:, head * head_width : (head + 1) * head_width]
+            )
+        return carry
+
+    lax.fori_loop(0, sequences, update, 0)
     for index in (3, 4, 5):
         loads[index].wait()
     shared_out = two_layer(token_rows, weights[3][...], weights[4][...], weights[5][...])
@@ -371,10 +414,12 @@
         + jnp.dot(low, picked, preferred_element_type=jnp.float32)
     )
     out_ref[...] = (after_float + rms_scale(combined, postfeed_ref[...])).astype(jnp.bfloat16)
-    drain(rows_buf.at[pl.ds(0, n - 1)], send_sems.at[0])
+    drain(rows_buf.at[pl.ds(0, chips - 1), 0], send_sems.at[0])
+    drain(rows_buf.at[:, 0], send_sems.at[8])
     drain(weight_buf.at[pl.ds(0, members - 1)], send_sems.at[1])
     drain(result_buf.at[pl.ds(0, n - 1)], send_sems.at[2])
-    drain(mix_buf.at[pl.ds(0, members - 1)], send_sems.at[3])
+    drain(mix_buf.at[pl.ds(0, near_chips - 1), 0], send_sems.at[3])
+    drain(mix_buf.at[:, 0], send_sems.at[9])
     drain(gated_buf.at[pl.ds(0, groups - 1)], send_sems.at[4])
     drain(mixed_buf.at[pl.ds(0, groups - 1)], send_sems.at[5])
     drain(arrived.at[pl.ds(0, n - 1)], send_sems.at[6])
@@ -395,20 +440,21 @@
     return pl.pallas_call(
         functools.partial(layer_kernel, n, groups),
         out_shape=(
-            jax.ShapeDtypeStruct((sequences, width), jnp.bfloat16),
-            jax.ShapeDtypeStruct((sequences, 4 * columns), jnp.float32),
-            jax.ShapeDtypeStruct((3, sequences, heads), jnp.float32),
+            pltpu.VMEM((sequences, width), jnp.bfloat16),
+            pltpu.VMEM(loads[8].shape, jnp.float32),
+            pltpu.VMEM((sequences, heads, head_width), jnp.float32),
+            pltpu.VMEM((sequences, heads), jnp.float32),
         ),
         in_specs=[VM] * len(small) + [ANY] * (len(projections) + len(loads)),
-        out_specs=(VM, VM, VM),
+        out_specs=(VM,) * 4,
         scratch_shapes=[pltpu.VMEM(w.shape, w.dtype) for w in loads]
         + [
             pieces,
-            narrow((n, sequences, width // groups)),
+            narrow((n // 2, 2, sequences, width // groups)),
             narrow((members, depth, wide)),
             narrow((n, sequences, wide)),
             narrow((n, sequences, wide)),
-            narrow((members,) + mix_weight.shape),
+            narrow((members // 2, 2) + mix_weight.shape),
             narrow((heads, sequences * head_width, 2 * head_width)),
             narrow((sequences, columns)),
             narrow((groups, sequences, columns)),
@@ -417,88 +463,44 @@
         ]
         + [slots] * 4
         + [
+            pltpu.VMEM((sequences, 4 * columns), jnp.float32),
+            pltpu.VMEM((2, sequences, heads), jnp.float32),
             pltpu.SemaphoreType.DMA((len(loads),)),
-            pltpu.SemaphoreType.DMA((8,)),
-            pltpu.SemaphoreType.DMA((8,)),
+            pltpu.SemaphoreType.DMA((10,)),
+            pltpu.SemaphoreType.DMA((10,)),
         ],
         compiler_params=pltpu.CompilerParams(
-            collective_id=0, has_side_effects=True, vmem_limit_bytes=56 * 1024 * 1024
+            collective_id=0, has_side_effects=True, vmem_limit_bytes=54 * 1024 * 1024
         ),
-    )(*small, *projections, *loads)
-
-
-def state_kernel(
-    tokens_ref,
-    projected_ref,
-    gates_ref,
-    normalizer_ref,
-    memory_ref,
-    next_tokens_ref,
-    next_memory_ref,
-    next_normalizer_ref,
-    next_stabilizer_ref,
-):
-    step = pl.program_id(0)
-    block, heads, head_width = memory_ref.shape[:3]
-    memory_width = heads * head_width
-    scale = head_width ** (-0.5)
-
-    @pl.when(step == 0)
-    def _():
-        next_tokens_ref[...] = tokens_ref[...]
-        next_stabilizer_ref[...] = gates_ref[2]
-        keep_all, write_all = gates_ref[0], gates_ref[1]
-        for head in range(heads):
-            start = memory_width + head * head_width
-            next_normalizer_ref[:, head, :] = keep_all[:, head : head + 1] * normalizer_ref[
-                :, head, :
-            ] + write_all[:, head : head + 1] * (
-                projected_ref[:, start : start + head_width] * scale
-            )
-
-    for item in range(block):
-        row = pl.ds(step * block + item, 1)
-        keep, write = gates_ref[0, row, :], gates_ref[1, row, :]
-        keys = projected_ref[row, memory_width : 2 * memory_width] * scale
-        values = projected_ref[row, 2 * memory_width : 3 * memory_width]
-        stacked = jnp.concatenate(
-            [
-                write[:, head : head + 1] * values[:, head * head_width : (head + 1) * head_width]
-                for head in range(heads)
-            ],
-            axis=0,
-        ).T
-        for head in range(heads):
-            next_memory_ref[item, head] = (
-                keep[:, head : head + 1] * memory_ref[item, head]
-                + stacked[:, head : head + 1]
-                * keys[:, head * head_width : (head + 1) * head_width]
-            )
-
-
-def write_state(tokens, projected, gates, normalizer, memory):
-    sequences = memory.shape[0]
-    steps = 4
-    block = (sequences // steps,) + memory.shape[1:]
-
-    def whole(array):
-        return pl.BlockSpec(array.shape, lambda i, rank=array.ndim: (0,) * rank)
-
-    moving = pl.BlockSpec(block, lambda i: (i, 0, 0, 0))
-    stabilizer = jax.ShapeDtypeStruct(gates.shape[1:], jnp.float32)
+    )(
+        *small,
+        *[pltpu.with_memory_space_constraint(w, pltpu.HBM) for w in projections + loads],
+    )
+
+
+def publish_kernel(*refs):
+    count = len(refs) // 2
+    sems = refs[-1]
+    copies = [
+        pltpu.make_async_copy(refs[index], refs[count + index], sems.at[index])
+        for index in range(count)
+    ]
+    for copy in copies:
+        copy.start()
+    for copy in copies:
+        copy.wait()
+
+
+def publish(*results):
+    held = [pltpu.with_memory_space_constraint(result, pltpu.VMEM) for result in results]
     return pl.pallas_call(
-        state_kernel,
-        grid=(steps,),
-        out_shape=(
-            jax.ShapeDtypeStruct(tokens.shape, tokens.dtype),
-            jax.ShapeDtypeStruct(memory.shape, memory.dtype),
-            jax.ShapeDtypeStruct(normalizer.shape, normalizer.dtype),
-            stabilizer,
-        ),
-        in_specs=[whole(tokens), whole(projected), whole(gates), whole(normalizer), moving],
-        out_specs=(whole(tokens), moving, whole(normalizer), whole(stabilizer)),
-        compiler_params=pltpu.CompilerParams(dimension_semantics=("arbitrary",)),
-    )(tokens, projected, gates, normalizer, memory)
+        publish_kernel,
+        out_shape=tuple(jax.ShapeDtypeStruct(r.shape, r.dtype) for r in results),
+        in_specs=[VM] * len(results),
+        out_specs=(ANY,) * len(results),
+        scratch_shapes=[pltpu.SemaphoreType.DMA((len(results),))],
+        compiler_params=pltpu.CompilerParams(vmem_limit_bytes=1024 * 1024),
+    )(*held)
 
 
 def on_device(
@@ -535,7 +537,7 @@
     capacity = min(
         sequences, max(2, 2 * ((sequences * choose_count + experts_total - 1) // experts_total))
     )
-    next_tokens, projected, gates = layer(
+    results = layer(
         devices,
         GROUPS,
         (
@@ -566,7 +568,7 @@
         ),
         capacity,
     )
-    return write_state(next_tokens, projected, gates, normalizer, memory_state)
+    return publish(*results)
 
 
 def solution(mesh):

time: 72.1 us -> 62.2 us (0.86)
  Pallas kernels: 71.2 us -> 61.4 us
    pallas_call x2, Pallas kernels: 71.2 us -> 61.4 us  [the longest x1 59.3 us: layer(): pl.pallas_call(functools.partial(layer_kernel, n, groups), out_shape=(plt...]
where the time goes in v1:
time: 62.2 us; the launch traced here: 62.1 us
  Pallas kernels  61.4 us (99%)
  between operations  0.65 us (1%)
    pallas_call x1, Pallas kernels, layer(): pl.pallas_call(functools.partial(layer_kernel, n, groups), out_shape=(plt...  59.3 us
    pallas_call x1, Pallas kernels, publish(): pl.pallas_call(publish_kernel, out_shape=tuple((jax.ShapeDtypeStruct(r.sh...  2.07 us

profile of v1, /device:TPU:29, one launch (start us, length us, event | category | flops | bytes accessed | tf_op | source)
XLA Modules:
  0.0 62.1 jit_solution(16609201955635991841)
XLA Ops:
  0.6 59.3 %shard_map.264 = (bf16[8,2048]{1,0:T(8,128)(2,1)S(1)}, f32[8,8,128,128]{3,2,1,0:T(8,128)S(1)}, f32[8,8,128]{2,1,0:T(8,128)S(1)}, f32[8,8]{1,0:T(8,128)S(1)}) custom-call(bf16[8,2048]{1,0:T(8,128)(2,1)} %refs_0_.1, f32[1,2048]{1,0:T(1,128)} %bitcast.12, f32[1,2048]{1,0:T(1,128)} %bitcast.13, f32[1,2048]{1,0:T(1,128)} %bitcast.14, f32[1,2048]{1,0:T(1,128)} %bitcast.15, ...), custom_call_target="tpu_custom_call" | custom-call | tf_op jit(solution)/shard_map/pallas_call | solution.py:440
  60.0 2.1 %shard_map.265 = (bf16[8,2048]{1,0:T(8,128)(2,1)}, f32[8,8,128,128]{3,2,1,0:T(8,128)}, f32[8,8,128]{2,1,0:T(8,128)}, f32[8,8]{1,0:T(8,128)}) custom-call(bf16[8,2048]{1,0:T(8,128)(2,1)S(1)} %get-tuple-element.8.refs_0_, f32[8,8,128,128]{3,2,1,0:T(8,128)S(1)} %get-tuple-element.9.refs_1_, f32[8,8,128]{2,1,0:T(8,128)S(1)} %get-tuple-element.10.refs_2_, ...), custom_call_target="tpu_custom_call" | custom-call | tf_op jit(solution)/shard_map/pallas_call | solution.py:496

commit v2 on v1

--- a/solution.py
+++ b/solution.py
@@ -10,6 +10,10 @@
 epsilon = 1e-06
 LANES = 128
 GROUPS = 4
+FAR_IN = 3
+FAR_OUT = 4
+CUBE = 8
+HALVES = 4
 MESH = pl.DeviceIdType.MESH
 VM = pl.BlockSpec(memory_space=pltpu.VMEM)
 ANY = pl.BlockSpec(memory_space=pl.ANY)
@@ -52,9 +56,20 @@
     pltpu.make_async_copy(ref, ref, sem).wait()
 
 
-def routing(ids, route_weights, slot_count, capacity):
+def flip(value, mask):
+    result, bit = value, 1
+    while bit <= mask:
+        if mask & bit:
+            result = result + bit * (1 - 2 * lax.rem(lax.div(value, bit), 2))
+        bit *= 2
+    return result
+
+
+def routing(ids, route_weights, first_slot, slot_count, capacity):
     sequences, choices = ids.shape
-    slot = lax.broadcasted_iota(jnp.int32, (sequences, slot_count), 1).astype(jnp.float32)
+    slot = (
+        first_slot + lax.broadcasted_iota(jnp.int32, (sequences, slot_count), 1)
+    ).astype(jnp.float32)
     owner = jnp.floor((slot + 0.5) * (1.0 / capacity))
     turn = slot - owner * capacity
     chosen = jnp.zeros((sequences, slot_count), jnp.float32)
@@ -78,14 +93,23 @@
     )
 
 
-def two_layer(rows, gate_weight, up_weight, down_weight):
+def gated_rows(rows, gate_weight, up_weight):
     gate_values = jnp.dot(rows, gate_weight, preferred_element_type=jnp.float32)
     up_values = jnp.dot(rows, up_weight, preferred_element_type=jnp.float32)
-    inner_rows = (gate_values * jax.nn.sigmoid(gate_values) * up_values).astype(jnp.bfloat16)
+    return (gate_values * jax.nn.sigmoid(gate_values) * up_values).astype(jnp.bfloat16)
+
+
+def two_layer(rows, gate_weight, up_weight, down_weight):
+    inner_rows = gated_rows(rows, gate_weight, up_weight)
     return jnp.dot(inner_rows, down_weight, preferred_element_type=jnp.float32)
 
 
 def layer_kernel(n, groups, *refs):
+    small_from = refs[:12]
+    projections = refs[12:16]
+    loads_from = refs[16:25]
+    out_ref, next_memory_ref, next_normalizer_ref, next_stabilizer_ref = refs[25:29]
+    small = refs[29:41]
     (
         tokens_ref,
         premix_ref,
@@ -99,14 +123,9 @@
         ids_ref,
         route_ref,
         mix_ref,
-        query_ref,
-        key_ref,
-        value_ref,
-        gate_ref,
-    ) = refs[:16]
-    loads_from = refs[16:25]
-    out_ref, next_memory_ref, next_normalizer_ref, next_stabilizer_ref = refs[25:29]
-    loaded = refs[29:38]
+    ) = small
+    staged = refs[41]
+    loaded = refs[42:51]
     (
         normed_buf,
         rows_buf,
@@ -123,12 +142,27 @@
         arrived,
         answer,
         returned,
+        line_rows,
+        near_out,
+        near_in,
+        near_answer,
+        near_back,
+        partial_out,
+        partial_in,
+        ids_line,
+        route_line,
+        dispatch_line,
+        combine_line,
         projected_ref,
         gates_ref,
+        small_sems,
+        staged_sems,
         load_sems,
         send_sems,
         recv_sems,
-    ) = refs[38:]
+        line_sems,
+        weight_sems,
+    ) = refs[51:]
     weights = loaded[:6]
     input_weight, forget_weight, memory = loaded[6:]
     me = lax.axis_index("ep")
@@ -138,27 +172,58 @@
     chip, core, near_chip = me // 2, lax.rem(me, 2), place // 2
     partner = me + 1 - 2 * core
     part_width = rows_buf.shape[3]
-    columns = weight_buf.shape[2]
-    per_matrix = query_ref.shape[1] // columns
+    halves, half_columns = weight_buf.shape[0], weight_buf.shape[3]
+    columns = halves * half_columns
+    per_matrix = staged.shape[2] // columns
     greet(n, me)
-    projections = (query_ref, key_ref, value_ref, gate_ref)
-
-    def column(block):
-        return pl.ds(pl.multiple_of(lax.rem(block, per_matrix) * columns, LANES), columns)
-
-    for index, ref in enumerate(projections):
-
-        @pl.when(place // per_matrix == index)
-        def _():
-            pltpu.make_async_copy(
-                ref.at[:, column(place)], weight_buf.at[place], recv_sems.at[1]
-            ).start()
-
-    pltpu.make_async_copy(mix_ref, mix_buf.at[near_chip, core], recv_sems.at[3]).start()
+    small_loads = [
+        pltpu.make_async_copy(source, target, small_sems.at[index])
+        for index, (source, target) in enumerate(zip(small_from, small))
+    ]
+    staged_loads = [
+        pltpu.make_async_copy(source, staged.at[index], staged_sems.at[index])
+        for index, source in enumerate(projections)
+    ]
+    for copy in small_loads[:2] + staged_loads + small_loads[2:]:
+        copy.start()
+    cubes = members // CUBE
+    UP, DOWN = range(groups), range(groups - 1, -1, -1)
+    cube, corner = lax.div(place, CUBE), lax.rem(place, CUBE)
+
+    def around(masks, body, include_own):
+        def one(i, carry):
+            base = lax.rem(cube + i, cubes) * CUBE
+            for mask in masks:
+                body(base + flip(corner, mask))
+            return carry
+
+        if not include_own:
+            for mask in masks:
+                if mask:
+                    body(cube * CUBE + flip(corner, mask))
+        lax.fori_loop(0 if include_own else 1, cubes, one, 0)
+
+    def each_near(body, step=1):
+        around(range(CUBE - step, -1, -step), body, False)
+
+    def each_peer(body, step=1, order=range(groups - 1, -1, -1)):
+        for mask in order:
+            peers = flip(plane, mask)
+            around(
+                range(CUBE - step, -1, -step),
+                lambda member: body(peers, member, peers * members + member),
+                mask > 0,
+            )
+    def column(block, half):
+        start = lax.rem(block, per_matrix) * columns + half * half_columns
+        return pl.ds(pl.multiple_of(start, LANES), half_columns)
+
     loads = [
         pltpu.make_async_copy(source, target, load_sems.at[index])
         for index, (source, target) in enumerate(zip(loads_from, loaded))
     ]
+    for copy in small_loads[:2]:
+        copy.wait()
     residual = tokens_ref[...].astype(jnp.float32)
     normed = rms_scale(residual, premix_ref[...]).astype(jnp.bfloat16)
     for group in range(groups):
@@ -166,37 +231,56 @@
     pltpu.make_async_copy(
         normed_buf.at[plane], rows_buf.at[chip, core], recv_sems.at[0]
     ).start()
+    for copy in staged_loads + small_loads[2:]:
+        copy.wait()
+    for half in range(halves):
+        pltpu.make_async_copy(
+            staged.at[lax.div(place, per_matrix), :, column(place, half)],
+            weight_buf.at[half, place],
+            weight_sems.at[half],
+        ).start()
+    pltpu.make_async_copy(mix_ref, mix_buf.at[near_chip, core], recv_sems.at[3]).start()
+    pltpu.make_async_copy(ids_ref, ids_line.at[plane], recv_sems.at[10]).start()
+    pltpu.make_async_copy(route_ref, route_line.at[plane], recv_sems.at[11]).start()
     greeted(n)
 
-    def send_rows(i, carry):
-        peer = lax.rem(me + 2 * i, n)
+    def send_rows(group, member, peer):
         send(
-            normed_buf.at[peer // members],
+            normed_buf.at[group],
             rows_buf.at[chip, core],
             send_sems.at[0],
             recv_sems.at[0],
             peer,
         )
-        return carry
-
-    def send_weights(i, carry):
-        block = lax.rem(place + i, members)
-        for index, ref in enumerate(projections):
-
-            @pl.when(block // per_matrix == index)
-            def _():
-                send(
-                    ref.at[:, column(block)],
-                    weight_buf.at[place],
-                    send_sems.at[1],
-                    recv_sems.at[1],
-                    plane * members + block,
-                )
-
-        return carry
-
-    lax.fori_loop(1, chips, send_rows, 0)
-    lax.fori_loop(1, members, send_weights, 0)
+
+    def line(source, target, stage):
+        for mask in range(groups - 1, 0, -1):
+            peer = flip(plane, mask)
+            send(
+                source(peer),
+                target.at[plane],
+                send_sems.at[stage],
+                recv_sems.at[stage],
+                peer * members + place,
+            )
+
+    def send_weights(half):
+        def one(block):
+            send(
+                staged.at[lax.div(block, per_matrix), :, column(block, half)],
+                weight_buf.at[half, place],
+                send_sems.at[1],
+                weight_sems.at[half],
+                plane * members + block,
+            )
+
+        each_near(one)
+
+    each_peer(send_rows, 2)
+    for half in range(halves):
+        send_weights(half)
+    line(lambda peer: ids_ref, ids_line, 10)
+    line(lambda peer: route_ref, route_line, 11)
     for index in (6, 7, 8, 3, 4, 5, 0, 1, 2):
         loads[index].start()
 
@@ -221,8 +305,12 @@
     gates_ref[0] = keep_old
     gates_ref[1] = write_new
     next_stabilizer_ref[...] = next_stabilizer
-    local, capacity, width = outgoing.shape[1:]
-    slots, combine = routing(ids_ref[...], route_ref[...], n * local * capacity, capacity)
+    local, capacity, far = outgoing.shape[1:]
+    width = tokens_ref.shape[1]
+    near = width - far
+    slot_count = n * local * capacity
+    near_slots = members * local * capacity
+    slots, combine = routing(ids_ref[...], route_ref[...], 0, slot_count, capacity)
     dispatch = slots.T.astype(jnp.bfloat16)
     sequences, heads, head_width = memory.shape[:3]
     loads[8].wait()
@@ -240,56 +328,60 @@
 
     lax.fori_loop(0, sequences, split, 0)
 
+    def exchange(source, target, stage, order):
+        def one(group, member, peer):
+            send(source.at[peer], target.at[me], send_sems.at[stage], recv_sems.at[stage], peer)
+
+        each_peer(one, 1, order)
+
     drain(rows_buf.at[:, core], recv_sems.at[0])
     send(
         rows_buf.at[:, core], rows_buf.at[:, core], send_sems.at[8], recv_sems.at[8], partner
     )
-    drain(weight_buf, recv_sems.at[1])
-    drain(rows_buf.at[:, 1 - core], recv_sems.at[8])
-    rows = rows_buf[...].reshape(n * rows_buf.shape[2], part_width)
-    weight = weight_buf[...].reshape(weight_buf.shape[0] * weight_buf.shape[1], columns)
-    product = jnp.dot(rows, weight, preferred_element_type=jnp.float32)
-    product_buf[...] = product.reshape(product_buf.shape).astype(jnp.bfloat16)
-    pltpu.make_async_copy(product_buf.at[me], result_buf.at[me], recv_sems.at[2]).start()
-
-    def exchange(source, target, stage):
-        def one(i, carry):
-            peer = lax.rem(me + i, n)
-            send(source.at[peer], target.at[me], send_sems.at[stage], recv_sems.at[stage], peer)
-            return carry
-
-        lax.fori_loop(1, n, one, 0)
-
-    def send_mix(i, carry):
+    for half in range(halves):
+        drain(weight_buf.at[half], weight_sems.at[half])
+        if half == 0:
+            drain(rows_buf.at[:, 1 - core], recv_sems.at[8])
+        rows = rows_buf[...].reshape(n * rows_buf.shape[2], part_width)
+        weight = weight_buf[half].reshape(members * weight_buf.shape[2], half_columns)
+        product = jnp.dot(rows, weight, preferred_element_type=jnp.float32)
+        product_buf[half] = product.reshape(product_buf.shape[1:]).astype(jnp.bfloat16)
+        pltpu.make_async_copy(
+            product_buf.at[half, me], result_buf.at[half, me], recv_sems.at[2]
+        ).start()
+        exchange(product_buf.at[half], result_buf.at[half], 2, DOWN)
+
+    def send_mix(member):
         send(
             mix_ref,
             mix_buf.at[near_chip, core],
             send_sems.at[3],
             recv_sems.at[3],
-            plane * members + lax.rem(place + 2 * i, members),
-        )
-        return carry
-
-    def line(source, target, stage):
-        for i in range(1, groups):
-            peer = lax.rem(plane + i, groups)
-            send(
-                source(peer),
-                target.at[plane],
-                send_sems.at[stage],
-                recv_sems.at[stage],
-                peer * members + place,
-            )
-
-    exchange(product_buf, result_buf, 2)
-    lax.fori_loop(1, near_chips, send_mix, 0)
+            plane * members + member,
+        )
+
+    each_near(send_mix, 2)
+    drain(ids_line, recv_sems.at[10])
+    drain(route_line, recv_sems.at[11])
+    for group in range(groups):
+        near_chosen, near_combine = routing(
+            ids_line[group], route_line[group], plane * near_slots, near_slots, capacity
+        )
+        dispatch_line[group] = near_chosen.T.astype(jnp.bfloat16)
+        near_high = near_combine.astype(jnp.bfloat16)
+        combine_line[group, :sequences] = near_high
+        combine_line[group, sequences:] = (
+            near_combine - near_high.astype(jnp.float32)
+        ).astype(jnp.bfloat16)
     drain(result_buf, recv_sems.at[2])
-    for member in range(members):
-        total = result_buf[member].astype(jnp.float32)
-        for group in range(1, groups):
-            total = total + result_buf[group * members + member].astype(jnp.float32)
-        total = total.astype(jnp.bfloat16).astype(jnp.float32)
-        projected_ref[:, member * columns : (member + 1) * columns] = total
+    for half in range(halves):
+        for member in range(members):
+            total = result_buf[half, member].astype(jnp.float32)
+            for group in range(1, groups):
+                total = total + result_buf[half, group * members + member].astype(jnp.float32)
+            total = total.astype(jnp.bfloat16).astype(jnp.float32)
+            start = member * columns + half * half_columns
+            projected_ref[:, start : start + half_columns] = total
     memory_width = heads * head_width
     row = lax.broadcasted_iota(jnp.int32, (sequences, head_width), 0)
     for head in range(heads):
@@ -323,35 +415,6 @@
 
     pltpu.make_async_copy(gated_src, gated_buf.at[plane], recv_sems.at[4]).start()
     line(lambda peer: gated_src, gated_buf, 4)
-    drain(mix_buf.at[:, core], recv_sems.at[3])
-    send(mix_buf.at[:, core], mix_buf.at[:, core], send_sems.at[9], recv_sems.at[9], partner)
-    drain(gated_buf, recv_sems.at[4])
-    drain(mix_buf.at[:, 1 - core], recv_sems.at[9])
-    gated = gated_buf[...].reshape(gated_buf.shape[0] * gated_buf.shape[1], gated_buf.shape[2])
-    mix_weight = mix_buf[...].reshape(members * mix_buf.shape[2], mix_buf.shape[3])
-    columns_buf[...] = (
-        lax.dot_general(
-            gated, mix_weight, (((1,), (1,)), ((), ())), preferred_element_type=jnp.float32
-        )
-        .reshape(columns_buf.shape)
-        .astype(jnp.bfloat16)
-    )
-    pltpu.make_async_copy(columns_buf.at[plane], mixed_buf.at[plane], recv_sems.at[5]).start()
-    line(lambda peer: columns_buf.at[peer], mixed_buf, 5)
-    drain(mixed_buf, recv_sems.at[5])
-    mixed = jnp.concatenate([mixed_buf[group] for group in range(groups)], axis=1)
-    after_mix = (residual + rms_scale(mixed.astype(jnp.float32), postmix_ref[...])).astype(
-        jnp.bfloat16
-    )
-    after_float = after_mix.astype(jnp.float32)
-    token_rows = rms_scale(after_float, prefeed_ref[...]).astype(jnp.bfloat16)
-    outgoing[...] = (
-        jnp.dot(dispatch, token_rows, preferred_element_type=jnp.float32)
-        .reshape(outgoing.shape)
-        .astype(jnp.bfloat16)
-    )
-    pltpu.make_async_copy(outgoing.at[me], arrived.at[me], recv_sems.at[6]).start()
-    exchange(outgoing, arrived, 6)
     key_scale = head_width ** (-0.5)
     for head in range(heads):
         start = memory_width + head * head_width
@@ -381,49 +444,173 @@
             )
         return carry
 
-    lax.fori_loop(0, sequences, update, 0)
+    lax.fori_loop(0, sequences // 2, update, 0)
+    drain(mix_buf.at[:, core], recv_sems.at[3])
+    send(mix_buf.at[:, core], mix_buf.at[:, core], send_sems.at[9], recv_sems.at[9], partner)
+    drain(gated_buf, recv_sems.at[4])
+    drain(mix_buf.at[:, 1 - core], recv_sems.at[9])
+    gated = gated_buf[...].reshape(gated_buf.shape[0] * gated_buf.shape[1], gated_buf.shape[2])
+    mix_weight = mix_buf[...].reshape(members * mix_buf.shape[2], mix_buf.shape[3])
+    columns_buf[...] = (
+        lax.dot_general(
+            gated, mix_weight, (((1,), (1,)), ((), ())), preferred_element_type=jnp.float32
+        )
+        .reshape(columns_buf.shape)
+        .astype(jnp.bfloat16)
+    )
+    pltpu.make_async_copy(columns_buf.at[plane], mixed_buf.at[plane], recv_sems.at[5]).start()
+    line(lambda peer: columns_buf.at[peer], mixed_buf, 5)
+    lax.fori_loop(sequences // 2, sequences, update, 0)
+    drain(mixed_buf, recv_sems.at[5])
+    mixed = jnp.concatenate([mixed_buf[group] for group in range(groups)], axis=1)
+    after_mix = (residual + rms_scale(mixed.astype(jnp.float32), postmix_ref[...])).astype(
+        jnp.bfloat16
+    )
+    after_float = after_mix.astype(jnp.float32)
+    token_rows = rms_scale(after_float, prefeed_ref[...]).astype(jnp.bfloat16)
+    line_rows[plane] = token_rows[:, far:]
+    for mask in range(groups - 1, 0, -1):
+        send(
+            line_rows.at[plane],
+            line_rows.at[plane],
+            send_sems.at[12],
+            line_sems.at[mask],
+            flip(plane, mask) * members + place,
+        )
+
+    def deal(group):
+        near_out[group] = (
+            jnp.dot(
+                dispatch_line[group], line_rows[group], preferred_element_type=jnp.float32
+            )
+            .reshape(near_out.shape[1:])
+            .astype(jnp.bfloat16)
+        )
+        pltpu.make_async_copy(
+            near_out.at[group, place], near_in.at[group, place], recv_sems.at[13]
+        ).start()
+
+        def one(member):
+            send(
+                near_out.at[group, member],
+                near_in.at[group, place],
+                send_sems.at[13],
+                recv_sems.at[13],
+                plane * members + member,
+            )
+
+        each_near(one)
+
+    deal(plane)
+    outgoing[...] = (
+        jnp.dot(dispatch, token_rows[:, :far], preferred_element_type=jnp.float32)
+        .reshape(outgoing.shape)
+        .astype(jnp.bfloat16)
+    )
+    pltpu.make_async_copy(outgoing.at[me], arrived.at[me], recv_sems.at[6]).start()
+    exchange(outgoing, arrived, 6, UP)
+    for mask in range(1, groups):
+        source = flip(plane, mask)
+        drain(line_rows.at[source], line_sems.at[mask])
+        deal(source)
     for index in (3, 4, 5):
         loads[index].wait()
     shared_out = two_layer(token_rows, weights[3][...], weights[4][...], weights[5][...])
     for index in (0, 1, 2):
         loads[index].wait()
+    drain(near_in, recv_sems.at[13])
     drain(arrived, recv_sems.at[6])
+    back = returned.shape[3]
+    inner_rows = []
     for item in range(local):
-        block = arrived[:, item].astype(jnp.float32).reshape(n * capacity, width)
+        block = jnp.concatenate(
+            [
+                arrived[:, item].astype(jnp.float32).reshape(n * capacity, far),
+                near_in[:, :, item].astype(jnp.float32).reshape(n * capacity, near),
+            ],
+            axis=1,
+        ).astype(jnp.bfloat16)
+        inner = gated_rows(block, weights[0][item], weights[1][item])
+        inner_rows.append(inner)
+        near_answer[:, :, item] = (
+            jnp.dot(inner, weights[2][item, :, back:], preferred_element_type=jnp.float32)
+            .reshape(groups, members, capacity, width - back)
+            .astype(jnp.bfloat16)
+        )
+    pltpu.make_async_copy(
+        near_answer.at[:, place], near_back.at[:, place], recv_sems.at[14]
+    ).start()
+
+    def send_back(member):
+        send(
+            near_answer.at[:, member],
+            near_back.at[:, place],
+            send_sems.at[14],
+            recv_sems.at[14],
+            plane * members + member,
+        )
+
+    each_near(send_back)
+    for item in range(local):
         answer[:, item] = (
-            two_layer(
-                block.astype(jnp.bfloat16),
-                weights[0][item],
-                weights[1][item],
-                weights[2][item],
+            jnp.dot(
+                inner_rows[item], weights[2][item, :, :back], preferred_element_type=jnp.float32
             )
-            .reshape(n, capacity, width)
+            .reshape(n, capacity, back)
             .astype(jnp.bfloat16)
         )
     pltpu.make_async_copy(answer.at[me], returned.at[me], recv_sems.at[7]).start()
-    exchange(answer, returned, 7)
+    exchange(answer, returned, 7, DOWN)
     high = combine.astype(jnp.bfloat16)
     low = (combine - high.astype(jnp.float32)).astype(jnp.bfloat16)
+    drain(near_back, recv_sems.at[14])
+
+    def weigh(group):
+        rows = near_back[group].astype(jnp.float32).reshape(near_slots, width - back)
+        both = jnp.dot(
+            combine_line[group], rows.astype(jnp.bfloat16), preferred_element_type=jnp.float32
+        )
+        return both[:sequences] + both[sequences:]
+
+    for i in range(groups - 1, 0, -1):
+        peer = flip(plane, i)
+        partial_out[peer] = weigh(peer).astype(jnp.bfloat16)
+        send(
+            partial_out.at[peer],
+            partial_in.at[i],
+            send_sems.at[15],
+            recv_sems.at[15],
+            peer * members + place,
+        )
+    near_sum = shared_out[:, back:] + weigh(plane)
     drain(returned, recv_sems.at[7])
-    picked = (
-        returned[...].astype(jnp.float32).reshape(combine.shape[1], width).astype(jnp.bfloat16)
-    )
-    combined = (
-        shared_out
+    picked = returned[...].astype(jnp.float32).reshape(slot_count, back).astype(jnp.bfloat16)
+    far_sum = (
+        shared_out[:, :back]
         + jnp.dot(high, picked, preferred_element_type=jnp.float32)
         + jnp.dot(low, picked, preferred_element_type=jnp.float32)
     )
+    drain(partial_in.at[pl.ds(1, groups - 1)], recv_sems.at[15])
+    for i in range(1, groups):
+        near_sum = near_sum + partial_in[i].astype(jnp.float32)
+    combined = jnp.concatenate([far_sum, near_sum], axis=1)
     out_ref[...] = (after_float + rms_scale(combined, postfeed_ref[...])).astype(jnp.bfloat16)
     drain(rows_buf.at[pl.ds(0, chips - 1), 0], send_sems.at[0])
     drain(rows_buf.at[:, 0], send_sems.at[8])
-    drain(weight_buf.at[pl.ds(0, members - 1)], send_sems.at[1])
-    drain(result_buf.at[pl.ds(0, n - 1)], send_sems.at[2])
+    drain(weight_buf.at[:, pl.ds(0, members - 1)], send_sems.at[1])
+    drain(result_buf.at[:, pl.ds(0, n - 1)], send_sems.at[2])
     drain(mix_buf.at[pl.ds(0, near_chips - 1), 0], send_sems.at[3])
     drain(mix_buf.at[:, 0], send_sems.at[9])
     drain(gated_buf.at[pl.ds(0, groups - 1)], send_sems.at[4])
     drain(mixed_buf.at[pl.ds(0, groups - 1)], send_sems.at[5])
     drain(arrived.at[pl.ds(0, n - 1)], send_sems.at[6])
     drain(returned.at[pl.ds(0, n - 1)], send_sems.at[7])
+    drain(ids_line.at[pl.ds(0, groups - 1)], send_sems.at[10])
+    drain(route_line.at[pl.ds(0, groups - 1)], send_sems.at[11])
+    drain(line_rows.at[pl.ds(0, groups - 1)], send_sems.at[12])
+    drain(near_in.at[:, pl.ds(0, members - 1)], send_sems.at[13])
+    drain(near_back.at[:, pl.ds(0, members - 1)], send_sems.at[14])
+    drain(partial_in.at[pl.ds(0, groups - 1)], send_sems.at[15])
 
 
 def layer(n, groups, small, projections, loads, capacity):
@@ -432,10 +619,24 @@
     depth, columns = projections[0].shape
     members = n // groups
     wide = 4 * columns // members
+    halves = max(1, min(HALVES, wide // LANES))
     local = loads[0].shape[0]
     heads, head_width = loads[8].shape[1:3]
     narrow = functools.partial(pltpu.VMEM, dtype=jnp.bfloat16)
-    slots = narrow((n, local, capacity, width))
+    far = width * FAR_IN // 8 // LANES * LANES
+    back = width * FAR_OUT // 8 // LANES * LANES
+    near_slots = members * local * capacity
+
+    def slots(size):
+        return [narrow((n, local, capacity, size))] * 2
+
+    def blocks(size):
+        return [narrow((groups, members, local, capacity, size))] * 2
+
+    def rows(size):
+        return [narrow((groups, sequences, size))]
+
+    choices = small[9].shape[1]
     pieces = narrow((groups, sequences, width // groups))
     return pl.pallas_call(
         functools.partial(layer_kernel, n, groups),
@@ -445,15 +646,17 @@
             pltpu.VMEM((sequences, heads, head_width), jnp.float32),
             pltpu.VMEM((sequences, heads), jnp.float32),
         ),
-        in_specs=[VM] * len(small) + [ANY] * (len(projections) + len(loads)),
+        in_specs=[ANY] * (len(small) + len(projections) + len(loads)),
         out_specs=(VM,) * 4,
-        scratch_shapes=[pltpu.VMEM(w.shape, w.dtype) for w in loads]
+        scratch_shapes=[pltpu.VMEM(w.shape, w.dtype) for w in small]
+        + [narrow((len(projections), depth, columns))]
+        + [pltpu.VMEM(w.shape, w.dtype) for w in loads]
         + [
             pieces,
             narrow((n // 2, 2, sequences, width // groups)),
-            narrow((members, depth, wide)),
-            narrow((n, sequences, wide)),
-            narrow((n, sequences, wide)),
+            narrow((halves, members, depth, wide // halves)),
+            narrow((halves, n, sequences, wide // halves)),
+            narrow((halves, n, sequences, wide // halves)),
             narrow((members // 2, 2) + mix_weight.shape),
             narrow((heads, sequences * head_width, 2 * head_width)),
             narrow((sequences, columns)),
@@ -461,20 +664,35 @@
             pieces,
             pieces,
         ]
-        + [slots] * 4
+        + slots(far)
+        + slots(back)
+        + rows(width - far)
+        + blocks(width - far)
+        + blocks(width - back)
+        + rows(width - back) * 2
         + [
+            pltpu.VMEM((groups, sequences, choices), jnp.int32),
+            pltpu.VMEM((groups, sequences, choices), jnp.float32),
+            narrow((groups, near_slots, sequences)),
+            narrow((groups, 2 * sequences, near_slots)),
             pltpu.VMEM((sequences, 4 * columns), jnp.float32),
             pltpu.VMEM((2, sequences, heads), jnp.float32),
+            pltpu.SemaphoreType.DMA((len(small),)),
+            pltpu.SemaphoreType.DMA((len(projections),)),
             pltpu.SemaphoreType.DMA((len(loads),)),
-            pltpu.SemaphoreType.DMA((10,)),
-            pltpu.SemaphoreType.DMA((10,)),
+            pltpu.SemaphoreType.DMA((16,)),
+            pltpu.SemaphoreType.DMA((16,)),
+            pltpu.SemaphoreType.DMA((groups,)),
+            pltpu.SemaphoreType.DMA((halves,)),
         ],
         compiler_params=pltpu.CompilerParams(
             collective_id=0, has_side_effects=True, vmem_limit_bytes=54 * 1024 * 1024
         ),
     )(
-        *small,
-        *[pltpu.with_memory_space_constraint(w, pltpu.HBM) for w in projections + loads],
+        *[
+            pltpu.with_memory_space_constraint(w, pltpu.HBM)
+            for w in small + projections + loads
+        ],
     )
 
 

time: 62.2 us -> 54.6 us (0.88)
  the two profiles are of different devices: /device:TPU:29 before, /device:TPU:0 now
where the time goes in v2:
time: 54.6 us; the launch traced here: 54.4 us
  Pallas kernels  53.8 us (99%)
  between operations  0.65 us (1%)
    pallas_call x1, Pallas kernels, layer(): pl.pallas_call(functools.partial(layer_kernel, n, groups), out_shape=(plt...  51.7 us
    pallas_call x1, Pallas kernels, publish(): pl.pallas_call(publish_kernel, out_shape=tuple((jax.ShapeDtypeStruct(r.sh...  2.07 us

profile of v2, /device:TPU:0, one launch (start us, length us, event | category | flops | bytes accessed | tf_op | source)
XLA Modules:
  0.0 54.4 jit_solution(14547267991646470109)
XLA Ops:
  0.6 51.7 %shard_map.264 = (bf16[8,2048]{1,0:T(8,128)(2,1)S(1)}, f32[8,8,128,128]{3,2,1,0:T(8,128)S(1)}, f32[8,8,128]{2,1,0:T(8,128)S(1)}, f32[8,8]{1,0:T(8,128)S(1)}) custom-call(bf16[8,2048]{1,0:T(8,128)(2,1)} %refs_0_.1, f32[1,2048]{1,0:T(1,128)} %bitcast.12, f32[1,2048]{1,0:T(1,128)} %bitcast.13, f32[1,2048]{1,0:T(1,128)} %bitcast.14, f32[1,2048]{1,0:T(1,128)} %bitcast.15, ...), custom_call_target="tpu_custom_call" | custom-call | tf_op jit(solution)/shard_map/pallas_call | solution.py:641
  52.4 2.1 %shard_map.265 = (bf16[8,2048]{1,0:T(8,128)(2,1)}, f32[8,8,128,128]{3,2,1,0:T(8,128)}, f32[8,8,128]{2,1,0:T(8,128)}, f32[8,8]{1,0:T(8,128)}) custom-call(bf16[8,2048]{1,0:T(8,128)(2,1)S(1)} %get-tuple-element.8.refs_0_, f32[8,8,128,128]{3,2,1,0:T(8,128)S(1)} %get-tuple-element.9.refs_1_, f32[8,8,128]{2,1,0:T(8,128)S(1)} %get-tuple-element.10.refs_2_, ...), custom_call_target="tpu_custom_call" | custom-call | tf_op jit(solution)/shard_map/pallas_call | solution.py:714

commit v3 on v2

--- a/solution.py
+++ b/solution.py
@@ -12,6 +12,9 @@
 GROUPS = 4
 FAR_IN = 3
 FAR_OUT = 4
+ROUNDS = 2
+CORNERS_IN = None
+CORNERS_OUT = range(8)
 CUBE = 8
 HALVES = 4
 MESH = pl.DeviceIdType.MESH
@@ -65,13 +68,13 @@
     return result
 
 
-def routing(ids, route_weights, first_slot, slot_count, capacity):
+def routing(ids, route_weights, first_slot, slot_count, capacity, first_turn):
     sequences, choices = ids.shape
     slot = (
         first_slot + lax.broadcasted_iota(jnp.int32, (sequences, slot_count), 1)
     ).astype(jnp.float32)
     owner = jnp.floor((slot + 0.5) * (1.0 / capacity))
-    turn = slot - owner * capacity
+    turn = slot - owner * capacity + first_turn
     chosen = jnp.zeros((sequences, slot_count), jnp.float32)
     weight_of = jnp.zeros((sequences, slot_count), jnp.float32)
     float_ids = ids.astype(jnp.float32)
@@ -153,6 +156,7 @@
         route_line,
         dispatch_line,
         combine_line,
+        near_sums,
         projected_ref,
         gates_ref,
         small_sems,
@@ -162,6 +166,12 @@
         recv_sems,
         line_sems,
         weight_sems,
+        result_sems,
+        mix_sems,
+        near_sems,
+        far_sems,
+        back_sems,
+        home_sems,
     ) = refs[51:]
     weights = loaded[:6]
     input_weight, forget_weight, memory = loaded[6:]
@@ -206,11 +216,11 @@
     def each_near(body, step=1):
         around(range(CUBE - step, -1, -step), body, False)
 
-    def each_peer(body, step=1, order=range(groups - 1, -1, -1)):
+    def each_peer(body, step=1, order=range(groups - 1, -1, -1), corners=None):
         for mask in order:
             peers = flip(plane, mask)
             around(
-                range(CUBE - step, -1, -step),
+                corners or range(CUBE - step, -1, -step),
                 lambda member: body(peers, member, peers * members + member),
                 mask > 0,
             )
@@ -239,7 +249,7 @@
             weight_buf.at[half, place],
             weight_sems.at[half],
         ).start()
-    pltpu.make_async_copy(mix_ref, mix_buf.at[near_chip, core], recv_sems.at[3]).start()
+    pltpu.make_async_copy(mix_ref, mix_buf.at[near_chip, core], mix_sems.at[near_chip]).start()
     pltpu.make_async_copy(ids_ref, ids_line.at[plane], recv_sems.at[10]).start()
     pltpu.make_async_copy(route_ref, route_line.at[plane], recv_sems.at[11]).start()
     greeted(n)
@@ -305,13 +315,18 @@
     gates_ref[0] = keep_old
     gates_ref[1] = write_new
     next_stabilizer_ref[...] = next_stabilizer
-    local, capacity, far = outgoing.shape[1:]
+    rounds, _, local, capacity, far = outgoing.shape
     width = tokens_ref.shape[1]
     near = width - far
     slot_count = n * local * capacity
     near_slots = members * local * capacity
-    slots, combine = routing(ids_ref[...], route_ref[...], 0, slot_count, capacity)
-    dispatch = slots.T.astype(jnp.bfloat16)
+    dispatch, combine = [], []
+    for turn in range(rounds):
+        slots, combined = routing(
+            ids_ref[...], route_ref[...], 0, slot_count, capacity, turn * capacity
+        )
+        dispatch.append(slots.T.astype(jnp.bfloat16))
+        combine.append(combined)
     sequences, heads, head_width = memory.shape[:3]
     loads[8].wait()
 
@@ -328,11 +343,12 @@
 
     lax.fori_loop(0, sequences, split, 0)
 
-    def exchange(source, target, stage, order):
+    def exchange(source, target, stage, order, corners=None, sem=None):
         def one(group, member, peer):
-            send(source.at[peer], target.at[me], send_sems.at[stage], recv_sems.at[stage], peer)
-
-        each_peer(one, 1, order)
+            send(source.at[peer], target.at[me], send_sems.at[stage], arrival, peer)
+
+        arrival = recv_sems.at[stage] if sem is None else sem
+        each_peer(one, 1, order, corners)
 
     drain(rows_buf.at[:, core], recv_sems.at[0])
     send(
@@ -347,34 +363,55 @@
         product = jnp.dot(rows, weight, preferred_element_type=jnp.float32)
         product_buf[half] = product.reshape(product_buf.shape[1:]).astype(jnp.bfloat16)
         pltpu.make_async_copy(
-            product_buf.at[half, me], result_buf.at[half, me], recv_sems.at[2]
+            product_buf.at[half, me], result_buf.at[half, me], result_sems.at[half]
         ).start()
-        exchange(product_buf.at[half], result_buf.at[half], 2, DOWN)
+        exchange(
+            product_buf.at[half], result_buf.at[half], 2, DOWN, None, result_sems.at[half]
+        )
 
     def send_mix(member):
         send(
             mix_ref,
             mix_buf.at[near_chip, core],
             send_sems.at[3],
-            recv_sems.at[3],
+            mix_sems.at[near_chip],
             plane * members + member,
         )
 
     each_near(send_mix, 2)
+
+    def forward_mix(member):
+        index = lax.div(member, 2)
+        drain(mix_buf.at[index, core], mix_sems.at[index])
+        send(
+            mix_buf.at[index, core],
+            mix_buf.at[index, core],
+            send_sems.at[9],
+            recv_sems.at[9],
+            partner,
+        )
+
+    forward_mix(place)
     drain(ids_line, recv_sems.at[10])
     drain(route_line, recv_sems.at[11])
-    for group in range(groups):
-        near_chosen, near_combine = routing(
-            ids_line[group], route_line[group], plane * near_slots, near_slots, capacity
-        )
-        dispatch_line[group] = near_chosen.T.astype(jnp.bfloat16)
-        near_high = near_combine.astype(jnp.bfloat16)
-        combine_line[group, :sequences] = near_high
-        combine_line[group, sequences:] = (
-            near_combine - near_high.astype(jnp.float32)
-        ).astype(jnp.bfloat16)
-    drain(result_buf, recv_sems.at[2])
+    for turn in range(rounds):
+        for group in range(groups):
+            near_chosen, near_combine = routing(
+                ids_line[group],
+                route_line[group],
+                plane * near_slots,
+                near_slots,
+                capacity,
+                turn * capacity,
+            )
+            dispatch_line[turn, group] = near_chosen.T.astype(jnp.bfloat16)
+            near_high = near_combine.astype(jnp.bfloat16)
+            combine_line[turn, group, :sequences] = near_high
+            combine_line[turn, group, sequences:] = (
+                near_combine - near_high.astype(jnp.float32)
+            ).astype(jnp.bfloat16)
     for half in range(halves):
+        drain(result_buf.at[half], result_sems.at[half])
         for member in range(members):
             total = result_buf[half, member].astype(jnp.float32)
             for group in range(1, groups):
@@ -445,8 +482,7 @@
         return carry
 
     lax.fori_loop(0, sequences // 2, update, 0)
-    drain(mix_buf.at[:, core], recv_sems.at[3])
-    send(mix_buf.at[:, core], mix_buf.at[:, core], send_sems.at[9], recv_sems.at[9], partner)
+    around(range(2, CUBE, 2), forward_mix, False)
     drain(gated_buf, recv_sems.at[4])
     drain(mix_buf.at[:, 1 - core], recv_sems.at[9])
     gated = gated_buf[...].reshape(gated_buf.shape[0] * gated_buf.shape[1], gated_buf.shape[2])
@@ -478,118 +514,154 @@
             flip(plane, mask) * members + place,
         )
 
-    def deal(group):
-        near_out[group] = (
+    def deal(turn, group):
+        near_out[turn, group] = (
             jnp.dot(
-                dispatch_line[group], line_rows[group], preferred_element_type=jnp.float32
-            )
-            .reshape(near_out.shape[1:])
+                dispatch_line[turn, group], line_rows[group], preferred_element_type=jnp.float32
+            )
+            .reshape(near_out.shape[2:])
             .astype(jnp.bfloat16)
         )
         pltpu.make_async_copy(
-            near_out.at[group, place], near_in.at[group, place], recv_sems.at[13]
+            near_out.at[turn, group, place], near_in.at[turn, group, place], near_sems.at[turn]
         ).start()
 
         def one(member):
             send(
-                near_out.at[group, member],
-                near_in.at[group, place],
+                near_out.at[turn, group, member],
+                near_in.at[turn, group, place],
                 send_sems.at[13],
-                recv_sems.at[13],
+                near_sems.at[turn],
                 plane * members + member,
             )
 
         each_near(one)
 
-    deal(plane)
-    outgoing[...] = (
-        jnp.dot(dispatch, token_rows[:, :far], preferred_element_type=jnp.float32)
-        .reshape(outgoing.shape)
-        .astype(jnp.bfloat16)
-    )
-    pltpu.make_async_copy(outgoing.at[me], arrived.at[me], recv_sems.at[6]).start()
-    exchange(outgoing, arrived, 6, UP)
+    def deal_far(turn):
+        outgoing[turn] = (
+            jnp.dot(dispatch[turn], token_rows[:, :far], preferred_element_type=jnp.float32)
+            .reshape(outgoing.shape[1:])
+            .astype(jnp.bfloat16)
+        )
+        pltpu.make_async_copy(
+            outgoing.at[turn, me], arrived.at[turn, me], far_sems.at[turn]
+        ).start()
+        exchange(
+            outgoing.at[turn], arrived.at[turn], 6, UP, CORNERS_IN, far_sems.at[turn]
+        )
+
+    deal(0, plane)
+    deal_far(0)
+    for turn in range(1, rounds):
+        deal(turn, plane)
     for mask in range(1, groups):
         source = flip(plane, mask)
         drain(line_rows.at[source], line_sems.at[mask])
-        deal(source)
+        deal(0, source)
+    for turn in range(1, rounds):
+        deal_far(turn)
+        for mask in range(1, groups):
+            deal(turn, flip(plane, mask))
     for index in (3, 4, 5):
         loads[index].wait()
     shared_out = two_layer(token_rows, weights[3][...], weights[4][...], weights[5][...])
     for index in (0, 1, 2):
         loads[index].wait()
-    drain(near_in, recv_sems.at[13])
-    drain(arrived, recv_sems.at[6])
-    back = returned.shape[3]
-    inner_rows = []
-    for item in range(local):
-        block = jnp.concatenate(
-            [
-                arrived[:, item].astype(jnp.float32).reshape(n * capacity, far),
-                near_in[:, :, item].astype(jnp.float32).reshape(n * capacity, near),
-            ],
-            axis=1,
-        ).astype(jnp.bfloat16)
-        inner = gated_rows(block, weights[0][item], weights[1][item])
-        inner_rows.append(inner)
-        near_answer[:, :, item] = (
-            jnp.dot(inner, weights[2][item, :, back:], preferred_element_type=jnp.float32)
-            .reshape(groups, members, capacity, width - back)
-            .astype(jnp.bfloat16)
-        )
-    pltpu.make_async_copy(
-        near_answer.at[:, place], near_back.at[:, place], recv_sems.at[14]
-    ).start()
-
-    def send_back(member):
-        send(
-            near_answer.at[:, member],
-            near_back.at[:, place],
-            send_sems.at[14],
-            recv_sems.at[14],
-            plane * members + member,
-        )
-
-    each_near(send_back)
-    for item in range(local):
-        answer[:, item] = (
-            jnp.dot(
-                inner_rows[item], weights[2][item, :, :back], preferred_element_type=jnp.float32
-            )
-            .reshape(n, capacity, back)
-            .astype(jnp.bfloat16)
-        )
-    pltpu.make_async_copy(answer.at[me], returned.at[me], recv_sems.at[7]).start()
-    exchange(answer, returned, 7, DOWN)
-    high = combine.astype(jnp.bfloat16)
-    low = (combine - high.astype(jnp.float32)).astype(jnp.bfloat16)
-    drain(near_back, recv_sems.at[14])
-
-    def weigh(group):
-        rows = near_back[group].astype(jnp.float32).reshape(near_slots, width - back)
+    back = returned.shape[4]
+    near = width - far
+
+    def work(turn):
+        drain(near_in.at[turn], near_sems.at[turn])
+        drain(arrived.at[turn], far_sems.at[turn])
+        inner_rows = []
+        for item in range(local):
+            block = jnp.concatenate(
+                [
+                    arrived[turn, :, item].astype(jnp.float32).reshape(slot_count // local, far),
+                    near_in[turn, :, :, item]
+                    .astype(jnp.float32)
+                    .reshape(slot_count // local, near),
+                ],
+                axis=1,
+            ).astype(jnp.bfloat16)
+            inner = gated_rows(block, weights[0][item], weights[1][item])
+            inner_rows.append(inner)
+            near_answer[turn, :, :, item] = (
+                jnp.dot(inner, weights[2][item, :, back:], preferred_element_type=jnp.float32)
+                .reshape(groups, members, capacity, width - back)
+                .astype(jnp.bfloat16)
+            )
+        pltpu.make_async_copy(
+            near_answer.at[turn, :, place], near_back.at[turn, :, place], back_sems.at[turn]
+        ).start()
+
+        def one(member):
+            send(
+                near_answer.at[turn, :, member],
+                near_back.at[turn, :, place],
+                send_sems.at[14],
+                back_sems.at[turn],
+                plane * members + member,
+            )
+
+        each_near(one)
+        for item in range(local):
+            answer[turn, :, item] = (
+                jnp.dot(
+                    inner_rows[item], weights[2][item, :, :back], preferred_element_type=jnp.float32
+                )
+                .reshape(n, capacity, back)
+                .astype(jnp.bfloat16)
+            )
+        pltpu.make_async_copy(
+            answer.at[turn, me], returned.at[turn, me], home_sems.at[turn]
+        ).start()
+        exchange(answer.at[turn], returned.at[turn], 7, DOWN, CORNERS_OUT, home_sems.at[turn])
+
+    def weigh(turn, group):
+        rows = near_back[turn, group].astype(jnp.float32).reshape(near_slots, width - back)
         both = jnp.dot(
-            combine_line[group], rows.astype(jnp.bfloat16), preferred_element_type=jnp.float32
+            combine_line[turn, group], rows.astype(jnp.bfloat16), preferred_element_type=jnp.float32
         )
         return both[:sequences] + both[sequences:]
 
-    for i in range(groups - 1, 0, -1):
+    def far_part(turn):
+        drain(returned.at[turn], home_sems.at[turn])
+        picked = returned[turn].astype(jnp.float32).reshape(slot_count, back).astype(jnp.bfloat16)
+        high = combine[turn].astype(jnp.bfloat16)
+        low = (combine[turn] - high.astype(jnp.float32)).astype(jnp.bfloat16)
+        return jnp.dot(high, picked, preferred_element_type=jnp.float32) + jnp.dot(
+            low, picked, preferred_element_type=jnp.float32
+        )
+
+    for turn in range(rounds):
+        work(turn)
+    last = rounds - 1
+    far_sum = shared_out[:, :back]
+    for turn in range(last):
+        drain(near_back.at[turn], back_sems.at[turn])
+        for i in range(groups):
+            peer = flip(plane, i)
+            known = weigh(turn, peer)
+            near_sums[i] = known if turn == 0 else near_sums[i] + known
+    drain(near_back.at[last], back_sems.at[last])
+    for i in range(groups - 1, -1, -1):
         peer = flip(plane, i)
-        partial_out[peer] = weigh(peer).astype(jnp.bfloat16)
-        send(
-            partial_out.at[peer],
-            partial_in.at[i],
-            send_sems.at[15],
-            recv_sems.at[15],
-            peer * members + place,
-        )
-    near_sum = shared_out[:, back:] + weigh(plane)
-    drain(returned, recv_sems.at[7])
-    picked = returned[...].astype(jnp.float32).reshape(slot_count, back).astype(jnp.bfloat16)
-    far_sum = (
-        shared_out[:, :back]
-        + jnp.dot(high, picked, preferred_element_type=jnp.float32)
-        + jnp.dot(low, picked, preferred_element_type=jnp.float32)
-    )
+        total = weigh(last, peer)
+        if last:
+            total = total + near_sums[i]
+        if i:
+            partial_out[peer] = total.astype(jnp.bfloat16)
+            send(
+                partial_out.at[peer],
+                partial_in.at[i],
+                send_sems.at[15],
+                recv_sems.at[15],
+                peer * members + place,
+            )
+    near_sum = shared_out[:, back:] + total
+    for turn in range(rounds):
+        far_sum = far_sum + far_part(turn)
     drain(partial_in.at[pl.ds(1, groups - 1)], recv_sems.at[15])
     for i in range(1, groups):
         near_sum = near_sum + partial_in[i].astype(jnp.float32)
@@ -603,13 +675,13 @@
     drain(mix_buf.at[:, 0], send_sems.at[9])
     drain(gated_buf.at[pl.ds(0, groups - 1)], send_sems.at[4])
     drain(mixed_buf.at[pl.ds(0, groups - 1)], send_sems.at[5])
-    drain(arrived.at[pl.ds(0, n - 1)], send_sems.at[6])
-    drain(returned.at[pl.ds(0, n - 1)], send_sems.at[7])
+    drain(arrived.at[:, pl.ds(0, n - 1)], send_sems.at[6])
+    drain(returned.at[:, pl.ds(0, n - 1)], send_sems.at[7])
     drain(ids_line.at[pl.ds(0, groups - 1)], send_sems.at[10])
     drain(route_line.at[pl.ds(0, groups - 1)], send_sems.at[11])
     drain(line_rows.at[pl.ds(0, groups - 1)], send_sems.at[12])
-    drain(near_in.at[:, pl.ds(0, members - 1)], send_sems.at[13])
-    drain(near_back.at[:, pl.ds(0, members - 1)], send_sems.at[14])
+    drain(near_in.at[:, :, pl.ds(0, members - 1)], send_sems.at[13])
+    drain(near_back.at[:, :, pl.ds(0, members - 1)], send_sems.at[14])
     drain(partial_in.at[pl.ds(0, groups - 1)], send_sems.at[15])
 
 
@@ -625,13 +697,15 @@
     narrow = functools.partial(pltpu.VMEM, dtype=jnp.bfloat16)
     far = width * FAR_IN // 8 // LANES * LANES
     back = width * FAR_OUT // 8 // LANES * LANES
+    rounds = ROUNDS if capacity % (2 * ROUNDS) == 0 else 1
+    capacity = capacity // rounds
     near_slots = members * local * capacity
 
     def slots(size):
-        return [narrow((n, local, capacity, size))] * 2
+        return [narrow((rounds, n, local, capacity, size))] * 2
 
     def blocks(size):
-        return [narrow((groups, members, local, capacity, size))] * 2
+        return [narrow((rounds, groups, members, local, capacity, size))] * 2
 
     def rows(size):
         return [narrow((groups, sequences, size))]
@@ -673,17 +747,24 @@
         + [
             pltpu.VMEM((groups, sequences, choices), jnp.int32),
             pltpu.VMEM((groups, sequences, choices), jnp.float32),
-            narrow((groups, near_slots, sequences)),
-            narrow((groups, 2 * sequences, near_slots)),
+            narrow((rounds, groups, near_slots, sequences)),
+            narrow((rounds, groups, 2 * sequences, near_slots)),
+            pltpu.VMEM((groups, sequences, width - back), jnp.float32),
             pltpu.VMEM((sequences, 4 * columns), jnp.float32),
             pltpu.VMEM((2, sequences, heads), jnp.float32),
             pltpu.SemaphoreType.DMA((len(small),)),
             pltpu.SemaphoreType.DMA((len(projections),)),
             pltpu.SemaphoreType.DMA((len(loads),)),
-            pltpu.SemaphoreType.DMA((16,)),
-            pltpu.SemaphoreType.DMA((16,)),
+            pltpu.SemaphoreType.DMA((18,)),
+            pltpu.SemaphoreType.DMA((18,)),
             pltpu.SemaphoreType.DMA((groups,)),
             pltpu.SemaphoreType.DMA((halves,)),
+            pltpu.SemaphoreType.DMA((halves,)),
+            pltpu.SemaphoreType.DMA((members // 2,)),
+            pltpu.SemaphoreType.DMA((rounds,)),
+            pltpu.SemaphoreType.DMA((rounds,)),
+            pltpu.SemaphoreType.DMA((rounds,)),
+            pltpu.SemaphoreType.DMA((rounds,)),
         ],
         compiler_params=pltpu.CompilerParams(
             collective_id=0, has_side_effects=True, vmem_limit_bytes=54 * 1024 * 1024

time: 54.6 us -> 53.9 us (0.987)
  Pallas kernels: 53.8 us -> 53.1 us
    pallas_call x1, Pallas kernels: 51.7 us -> 51 us  [layer(): pl.pallas_call(functools.partial(layer_kernel, n, groups), out_shape=(plt...]
where the time goes in v3:
time: 53.9 us; the launch traced here: 53.8 us
  Pallas kernels  53.1 us (99%)
  between operations  0.65 us (1%)
    pallas_call x1, Pallas kernels, layer(): pl.pallas_call(functools.partial(layer_kernel, n, groups), out_shape=(plt...  51 us
    pallas_call x1, Pallas kernels, publish(): pl.pallas_call(publish_kernel, out_shape=tuple((jax.ShapeDtypeStruct(r.sh...  2.07 us

profile of v3, /device:TPU:0, one launch (start us, length us, event | category | flops | bytes accessed | tf_op | source)
XLA Modules:
  0.0 53.8 jit_solution(12153793087644152599)
XLA Ops:
  0.6 51.0 %shard_map.264 = (bf16[8,2048]{1,0:T(8,128)(2,1)S(1)}, f32[8,8,128,128]{3,2,1,0:T(8,128)S(1)}, f32[8,8,128]{2,1,0:T(8,128)S(1)}, f32[8,8]{1,0:T(8,128)S(1)}) custom-call(bf16[8,2048]{1,0:T(8,128)(2,1)} %refs_0_.1, f32[1,2048]{1,0:T(1,128)} %bitcast.12, f32[1,2048]{1,0:T(1,128)} %bitcast.13, f32[1,2048]{1,0:T(1,128)} %bitcast.14, f32[1,2048]{1,0:T(1,128)} %bitcast.15, ...), custom_call_target="tpu_custom_call" | custom-call | tf_op jit(solution)/shard_map/pallas_call | solution.py:715
  51.7 2.1 %shard_map.265 = (bf16[8,2048]{1,0:T(8,128)(2,1)}, f32[8,8,128,128]{3,2,1,0:T(8,128)}, f32[8,8,128]{2,1,0:T(8,128)}, f32[8,8]{1,0:T(8,128)}) custom-call(bf16[8,2048]{1,0:T(8,128)(2,1)S(1)} %get-tuple-element.8.refs_0_, f32[8,8,128,128]{3,2,1,0:T(8,128)S(1)} %get-tuple-element.9.refs_1_, f32[8,8,128]{2,1,0:T(8,128)S(1)} %get-tuple-element.10.refs_2_, ...), custom_call_target="tpu_custom_call" | custom-call | tf_op jit(solution)/shard_map/pallas_call | solution.py:795

commit v4 on v3

--- a/solution.py
+++ b/solution.py
@@ -10,11 +10,9 @@
 epsilon = 1e-06
 LANES = 128
 GROUPS = 4
-FAR_IN = 3
+FAR_IN = 4
 FAR_OUT = 4
 ROUNDS = 2
-CORNERS_IN = None
-CORNERS_OUT = range(8)
 CUBE = 8
 HALVES = 4
 MESH = pl.DeviceIdType.MESH
@@ -159,10 +157,12 @@
         near_sums,
         projected_ref,
         gates_ref,
+        sent,
         small_sems,
-        staged_sems,
+        staged_sem,
         load_sems,
-        send_sems,
+        send_sem,
+        route_sem,
         recv_sems,
         line_sems,
         weight_sems,
@@ -191,7 +191,7 @@
         for index, (source, target) in enumerate(zip(small_from, small))
     ]
     staged_loads = [
-        pltpu.make_async_copy(source, staged.at[index], staged_sems.at[index])
+        pltpu.make_async_copy(source, staged.at[index], staged_sem)
         for index, source in enumerate(projections)
     ]
     for copy in small_loads[:2] + staged_loads + small_loads[2:]:
@@ -241,8 +241,46 @@
     pltpu.make_async_copy(
         normed_buf.at[plane], rows_buf.at[chip, core], recv_sems.at[0]
     ).start()
-    for copy in staged_loads + small_loads[2:]:
+    drain(staged, staged_sem)
+    for copy in small_loads[2:]:
         copy.wait()
+    greeted(n)
+
+    def send_rows(group, member, peer):
+        send(
+            normed_buf.at[group],
+            rows_buf.at[chip, core],
+            send_sem,
+            recv_sems.at[0],
+            peer,
+        )
+
+    def line(source, target, stage, leave=None):
+        for mask in range(groups - 1, 0, -1):
+            peer = flip(plane, mask)
+            send(
+                source(peer),
+                target.at[plane],
+                send_sem if leave is None else leave,
+                recv_sems.at[stage],
+                peer * members + place,
+            )
+
+    def send_weights(half):
+        def one(block):
+            send(
+                staged.at[lax.div(block, per_matrix), :, column(block, half)],
+                weight_buf.at[half, place],
+                send_sem,
+                weight_sems.at[half],
+                plane * members + block,
+            )
+
+        each_near(one)
+
+    each_peer(send_rows, 2)
+    for half in range(halves):
+        send_weights(half)
     for half in range(halves):
         pltpu.make_async_copy(
             staged.at[lax.div(place, per_matrix), :, column(place, half)],
@@ -250,47 +288,10 @@
             weight_sems.at[half],
         ).start()
     pltpu.make_async_copy(mix_ref, mix_buf.at[near_chip, core], mix_sems.at[near_chip]).start()
-    pltpu.make_async_copy(ids_ref, ids_line.at[plane], recv_sems.at[10]).start()
-    pltpu.make_async_copy(route_ref, route_line.at[plane], recv_sems.at[11]).start()
-    greeted(n)
-
-    def send_rows(group, member, peer):
-        send(
-            normed_buf.at[group],
-            rows_buf.at[chip, core],
-            send_sems.at[0],
-            recv_sems.at[0],
-            peer,
-        )
-
-    def line(source, target, stage):
-        for mask in range(groups - 1, 0, -1):
-            peer = flip(plane, mask)
-            send(
-                source(peer),
-                target.at[plane],
-                send_sems.at[stage],
-                recv_sems.at[stage],
-                peer * members + place,
-            )
-
-    def send_weights(half):
-        def one(block):
-            send(
-                staged.at[lax.div(block, per_matrix), :, column(block, half)],
-                weight_buf.at[half, place],
-                send_sems.at[1],
-                weight_sems.at[half],
-                plane * members + block,
-            )
-
-        each_near(one)
-
-    each_peer(send_rows, 2)
-    for half in range(halves):
-        send_weights(half)
-    line(lambda peer: ids_ref, ids_line, 10)
-    line(lambda peer: route_ref, route_line, 11)
+    pltpu.make_async_copy(ids_ref, ids_line.at[plane], recv_sems.at[5]).start()
+    pltpu.make_async_copy(route_ref, route_line.at[plane], recv_sems.at[6]).start()
+    line(lambda peer: ids_ref, ids_line, 5, line_sems.at[0])
+    line(lambda peer: route_ref, route_line, 6, route_sem)
     for index in (6, 7, 8, 3, 4, 5, 0, 1, 2):
         loads[index].start()
 
@@ -343,21 +344,20 @@
 
     lax.fori_loop(0, sequences, split, 0)
 
-    def exchange(source, target, stage, order, corners=None, sem=None):
+    def exchange(source, target, arrival, order, corners=None):
         def one(group, member, peer):
-            send(source.at[peer], target.at[me], send_sems.at[stage], arrival, peer)
-
-        arrival = recv_sems.at[stage] if sem is None else sem
+            send(source.at[peer], target.at[me], send_sem, arrival, peer)
+
         each_peer(one, 1, order, corners)
 
     drain(rows_buf.at[:, core], recv_sems.at[0])
     send(
-        rows_buf.at[:, core], rows_buf.at[:, core], send_sems.at[8], recv_sems.at[8], partner
+        rows_buf.at[:, core], rows_buf.at[:, core], send_sem, recv_sems.at[3], partner
     )
     for half in range(halves):
         drain(weight_buf.at[half], weight_sems.at[half])
         if half == 0:
-            drain(rows_buf.at[:, 1 - core], recv_sems.at[8])
+            drain(rows_buf.at[:, 1 - core], recv_sems.at[3])
         rows = rows_buf[...].reshape(n * rows_buf.shape[2], part_width)
         weight = weight_buf[half].reshape(members * weight_buf.shape[2], half_columns)
         product = jnp.dot(rows, weight, preferred_element_type=jnp.float32)
@@ -365,15 +365,13 @@
         pltpu.make_async_copy(
             product_buf.at[half, me], result_buf.at[half, me], result_sems.at[half]
         ).start()
-        exchange(
-            product_buf.at[half], result_buf.at[half], 2, DOWN, None, result_sems.at[half]
-        )
+        exchange(product_buf.at[half], result_buf.at[half], result_sems.at[half], DOWN)
 
     def send_mix(member):
         send(
             mix_ref,
             mix_buf.at[near_chip, core],
-            send_sems.at[3],
+            send_sem,
             mix_sems.at[near_chip],
             plane * members + member,
         )
@@ -386,14 +384,14 @@
         send(
             mix_buf.at[index, core],
             mix_buf.at[index, core],
-            send_sems.at[9],
-            recv_sems.at[9],
+            send_sem,
+            recv_sems.at[4],
             partner,
         )
 
     forward_mix(place)
-    drain(ids_line, recv_sems.at[10])
-    drain(route_line, recv_sems.at[11])
+    drain(ids_line, recv_sems.at[5])
+    drain(route_line, recv_sems.at[6])
     for turn in range(rounds):
         for group in range(groups):
             near_chosen, near_combine = routing(
@@ -410,6 +408,37 @@
             combine_line[turn, group, sequences:] = (
                 near_combine - near_high.astype(jnp.float32)
             ).astype(jnp.bfloat16)
+    memory_width = heads * head_width
+    row = lax.broadcasted_iota(jnp.int32, (sequences, head_width), 0)
+
+    def read_head(head):
+        def piece(matrix):
+            start = matrix * memory_width + head * head_width
+            return projected_ref[:, start : start + head_width]
+
+        span = slice(head * head_width, (head + 1) * head_width)
+        query, value, out_gate = piece(0), piece(2), piece(3)
+        key = piece(1) * head_width ** (-0.5)
+        keep, write = keep_old[:, head : head + 1], write_new[:, head : head + 1]
+        local_score = write * jnp.sum(query * key, axis=-1, keepdims=True)
+        denominator = (
+            keep * jnp.sum(normalizer_ref[:, head, :] * query, axis=-1, keepdims=True) + local_score
+        )
+        narrow = query.astype(jnp.bfloat16)
+        reads = lax.dot_general(
+            jnp.concatenate([narrow, narrow], axis=1),
+            split_buf[head],
+            (((1,), (1,)), ((), ())),
+            preferred_element_type=jnp.float32,
+        )
+        read = jnp.zeros((sequences, head_width), jnp.float32)
+        for s in range(sequences):
+            read = jnp.where(row == s, reads[:, s * head_width : (s + 1) * head_width], read)
+        memory_read = (keep * read + local_score * value) / jnp.maximum(
+            jnp.abs(denominator), 1.0
+        )
+        gated_src[:, span] = (jax.nn.sigmoid(out_gate) * memory_read).astype(jnp.bfloat16)
+
     for half in range(halves):
         drain(result_buf.at[half], result_sems.at[half])
         for member in range(members):
@@ -419,39 +448,12 @@
             total = total.astype(jnp.bfloat16).astype(jnp.float32)
             start = member * columns + half * half_columns
             projected_ref[:, start : start + half_columns] = total
-    memory_width = heads * head_width
-    row = lax.broadcasted_iota(jnp.int32, (sequences, head_width), 0)
-    for head in range(heads):
-
-        def piece(matrix):
-            start = matrix * memory_width + head * head_width
-            return projected_ref[:, start : start + head_width]
-
-        span = slice(head * head_width, (head + 1) * head_width)
-        query, value, out_gate = piece(0), piece(2), piece(3)
-        key = piece(1) * head_width ** (-0.5)
-        keep, write = keep_old[:, head : head + 1], write_new[:, head : head + 1]
-        local_score = write * jnp.sum(query * key, axis=-1, keepdims=True)
-        denominator = (
-            keep * jnp.sum(normalizer_ref[:, head, :] * query, axis=-1, keepdims=True) + local_score
-        )
-        narrow = query.astype(jnp.bfloat16)
-        reads = lax.dot_general(
-            jnp.concatenate([narrow, narrow], axis=1),
-            split_buf[head],
-            (((1,), (1,)), ((), ())),
-            preferred_element_type=jnp.float32,
-        )
-        read = jnp.zeros((sequences, head_width), jnp.float32)
-        for s in range(sequences):
-            read = jnp.where(row == s, reads[:, s * head_width : (s + 1) * head_width], read)
-        memory_read = (keep * read + local_score * value) / jnp.maximum(
-            jnp.abs(denominator), 1.0
-        )
-        gated_src[:, span] = (jax.nn.sigmoid(out_gate) * memory_read).astype(jnp.bfloat16)
-
-    pltpu.make_async_copy(gated_src, gated_buf.at[plane], recv_sems.at[4]).start()
-    line(lambda peer: gated_src, gated_buf, 4)
+        for head in range(heads):
+            if head * head_width % columns // half_columns == half:
+                read_head(head)
+
+    pltpu.make_async_copy(gated_src, gated_buf.at[plane], recv_sems.at[1]).start()
+    line(lambda peer: gated_src, gated_buf, 1)
     key_scale = head_width ** (-0.5)
     for head in range(heads):
         start = memory_width + head * head_width
@@ -483,8 +485,8 @@
 
     lax.fori_loop(0, sequences // 2, update, 0)
     around(range(2, CUBE, 2), forward_mix, False)
-    drain(gated_buf, recv_sems.at[4])
-    drain(mix_buf.at[:, 1 - core], recv_sems.at[9])
+    drain(gated_buf, recv_sems.at[1])
+    drain(mix_buf.at[:, 1 - core], recv_sems.at[4])
     gated = gated_buf[...].reshape(gated_buf.shape[0] * gated_buf.shape[1], gated_buf.shape[2])
     mix_weight = mix_buf[...].reshape(members * mix_buf.shape[2], mix_buf.shape[3])
     columns_buf[...] = (
@@ -494,10 +496,10 @@
         .reshape(columns_buf.shape)
         .astype(jnp.bfloat16)
     )
-    pltpu.make_async_copy(columns_buf.at[plane], mixed_buf.at[plane], recv_sems.at[5]).start()
-    line(lambda peer: columns_buf.at[peer], mixed_buf, 5)
+    pltpu.make_async_copy(columns_buf.at[plane], mixed_buf.at[plane], recv_sems.at[2]).start()
+    line(lambda peer: columns_buf.at[peer], mixed_buf, 2)
     lax.fori_loop(sequences // 2, sequences, update, 0)
-    drain(mixed_buf, recv_sems.at[5])
+    drain(mixed_buf, recv_sems.at[2])
     mixed = jnp.concatenate([mixed_buf[group] for group in range(groups)], axis=1)
     after_mix = (residual + rms_scale(mixed.astype(jnp.float32), postmix_ref[...])).astype(
         jnp.bfloat16
@@ -509,7 +511,7 @@
         send(
             line_rows.at[plane],
             line_rows.at[plane],
-            send_sems.at[12],
+            send_sem,
             line_sems.at[mask],
             flip(plane, mask) * members + place,
         )
@@ -530,7 +532,7 @@
             send(
                 near_out.at[turn, group, member],
                 near_in.at[turn, group, place],
-                send_sems.at[13],
+                send_sem,
                 near_sems.at[turn],
                 plane * members + member,
             )
@@ -546,9 +548,7 @@
         pltpu.make_async_copy(
             outgoing.at[turn, me], arrived.at[turn, me], far_sems.at[turn]
         ).start()
-        exchange(
-            outgoing.at[turn], arrived.at[turn], 6, UP, CORNERS_IN, far_sems.at[turn]
-        )
+        exchange(outgoing.at[turn], arrived.at[turn], far_sems.at[turn], UP, range(CUBE))
 
     deal(0, plane)
     deal_far(0)
@@ -599,12 +599,15 @@
             send(
                 near_answer.at[turn, :, member],
                 near_back.at[turn, :, place],
-                send_sems.at[14],
+                send_sem,
                 back_sems.at[turn],
                 plane * members + member,
             )
 
         each_near(one)
+        return inner_rows
+
+    def work_far(turn, inner_rows):
         for item in range(local):
             answer[turn, :, item] = (
                 jnp.dot(
@@ -616,7 +619,7 @@
         pltpu.make_async_copy(
             answer.at[turn, me], returned.at[turn, me], home_sems.at[turn]
         ).start()
-        exchange(answer.at[turn], returned.at[turn], 7, DOWN, CORNERS_OUT, home_sems.at[turn])
+        exchange(answer.at[turn], returned.at[turn], home_sems.at[turn], DOWN, range(CUBE))
 
     def weigh(turn, group):
         rows = near_back[turn, group].astype(jnp.float32).reshape(near_slots, width - back)
@@ -635,7 +638,7 @@
         )
 
     for turn in range(rounds):
-        work(turn)
+        work_far(turn, work(turn))
     last = rounds - 1
     far_sum = shared_out[:, :back]
     for turn in range(last):
@@ -652,37 +655,26 @@
             total = total + near_sums[i]
         if i:
             partial_out[peer] = total.astype(jnp.bfloat16)
-            send(
-                partial_out.at[peer],
-                partial_in.at[i],
-                send_sems.at[15],
-                recv_sems.at[15],
-                peer * members + place,
-            )
+    for i in range(groups - 1, 0, -1):
+        peer = flip(plane, i)
+        send(
+            partial_out.at[peer],
+            partial_in.at[i],
+            send_sem,
+            recv_sems.at[7],
+            peer * members + place,
+        )
     near_sum = shared_out[:, back:] + total
     for turn in range(rounds):
         far_sum = far_sum + far_part(turn)
-    drain(partial_in.at[pl.ds(1, groups - 1)], recv_sems.at[15])
+    drain(partial_in.at[pl.ds(1, groups - 1)], recv_sems.at[7])
     for i in range(1, groups):
         near_sum = near_sum + partial_in[i].astype(jnp.float32)
     combined = jnp.concatenate([far_sum, near_sum], axis=1)
     out_ref[...] = (after_float + rms_scale(combined, postfeed_ref[...])).astype(jnp.bfloat16)
-    drain(rows_buf.at[pl.ds(0, chips - 1), 0], send_sems.at[0])
-    drain(rows_buf.at[:, 0], send_sems.at[8])
-    drain(weight_buf.at[:, pl.ds(0, members - 1)], send_sems.at[1])
-    drain(result_buf.at[:, pl.ds(0, n - 1)], send_sems.at[2])
-    drain(mix_buf.at[pl.ds(0, near_chips - 1), 0], send_sems.at[3])
-    drain(mix_buf.at[:, 0], send_sems.at[9])
-    drain(gated_buf.at[pl.ds(0, groups - 1)], send_sems.at[4])
-    drain(mixed_buf.at[pl.ds(0, groups - 1)], send_sems.at[5])
-    drain(arrived.at[:, pl.ds(0, n - 1)], send_sems.at[6])
-    drain(returned.at[:, pl.ds(0, n - 1)], send_sems.at[7])
-    drain(ids_line.at[pl.ds(0, groups - 1)], send_sems.at[10])
-    drain(route_line.at[pl.ds(0, groups - 1)], send_sems.at[11])
-    drain(line_rows.at[pl.ds(0, groups - 1)], send_sems.at[12])
-    drain(near_in.at[:, :, pl.ds(0, members - 1)], send_sems.at[13])
-    drain(near_back.at[:, :, pl.ds(0, members - 1)], send_sems.at[14])
-    drain(partial_in.at[pl.ds(0, groups - 1)], send_sems.at[15])
+    drain(sent, send_sem)
+    drain(ids_line.at[pl.ds(0, groups - 1)], line_sems.at[0])
+    drain(route_line.at[pl.ds(0, groups - 1)], route_sem)
 
 
 def layer(n, groups, small, projections, loads, capacity):
@@ -700,6 +692,18 @@
     rounds = ROUNDS if capacity % (2 * ROUNDS) == 0 else 1
     capacity = capacity // rounds
     near_slots = members * local * capacity
+
+    chips, near_chips = n // 2, members // 2
+    slot_rows = rounds * local * capacity
+    sent = (
+        (2 * chips - 1) * sequences * (width // groups)
+        + (members - 1) * depth * wide
+        + (n - 1) * sequences * wide
+        + (2 * near_chips - 1) * mix_weight.size
+        + (groups - 1) * sequences * (columns + width // groups + 2 * width - far - back)
+        + (n - 1) * slot_rows * (far + back)
+        + groups * (members - 1) * slot_rows * (2 * width - far - back)
+    )
 
     def slots(size):
         return [narrow((rounds, n, local, capacity, size))] * 2
@@ -752,11 +756,13 @@
             pltpu.VMEM((groups, sequences, width - back), jnp.float32),
             pltpu.VMEM((sequences, 4 * columns), jnp.float32),
             pltpu.VMEM((2, sequences, heads), jnp.float32),
+            narrow((sent // LANES, LANES)),
             pltpu.SemaphoreType.DMA((len(small),)),
-            pltpu.SemaphoreType.DMA((len(projections),)),
+            pltpu.SemaphoreType.DMA,
             pltpu.SemaphoreType.DMA((len(loads),)),
-            pltpu.SemaphoreType.DMA((18,)),
-            pltpu.SemaphoreType.DMA((18,)),
+            pltpu.SemaphoreType.DMA,
+            pltpu.SemaphoreType.DMA,
+            pltpu.SemaphoreType.DMA((8,)),
             pltpu.SemaphoreType.DMA((groups,)),
             pltpu.SemaphoreType.DMA((halves,)),
             pltpu.SemaphoreType.DMA((halves,)),

time: 53.9 us -> 53.3 us (0.989)
  Pallas kernels: 53.1 us -> 52.5 us
    pallas_call x1, Pallas kernels: 51 us -> 50.4 us  [layer(): pl.pallas_call(functools.partial(layer_kernel, n, groups), out_shape=(plt...]
where the time goes in v4:
time: 53.3 us; the launch traced here: 53.2 us
  Pallas kernels  52.5 us (98%)
  between operations  0.65 us (1%)
    pallas_call x1, Pallas kernels, layer(): pl.pallas_call(functools.partial(layer_kernel, n, groups), out_shape=(plt...  50.4 us
    pallas_call x1, Pallas kernels, publish(): pl.pallas_call(publish_kernel, out_shape=tuple((jax.ShapeDtypeStruct(r.sh...  2.07 us

profile of v4, /device:TPU:0, one launch (start us, length us, event | category | flops | bytes accessed | tf_op | source)
XLA Modules:
  0.0 53.2 jit_solution(2920009808225924941)
XLA Ops:
  0.6 50.4 %shard_map.264 = (bf16[8,2048]{1,0:T(8,128)(2,1)S(1)}, f32[8,8,128,128]{3,2,1,0:T(8,128)S(1)}, f32[8,8,128]{2,1,0:T(8,128)S(1)}, f32[8,8]{1,0:T(8,128)S(1)}) custom-call(bf16[8,2048]{1,0:T(8,128)(2,1)} %refs_0_.1, f32[1,2048]{1,0:T(1,128)} %bitcast.12, f32[1,2048]{1,0:T(1,128)} %bitcast.13, f32[1,2048]{1,0:T(1,128)} %bitcast.14, f32[1,2048]{1,0:T(1,128)} %bitcast.15, ...), custom_call_target="tpu_custom_call" | custom-call | tf_op jit(solution)/shard_map/pallas_call | solution.py:719
  51.1 2.1 %shard_map.265 = (bf16[8,2048]{1,0:T(8,128)(2,1)}, f32[8,8,128,128]{3,2,1,0:T(8,128)}, f32[8,8,128]{2,1,0:T(8,128)}, f32[8,8]{1,0:T(8,128)}) custom-call(bf16[8,2048]{1,0:T(8,128)(2,1)S(1)} %get-tuple-element.8.refs_0_, f32[8,8,128,128]{3,2,1,0:T(8,128)S(1)} %get-tuple-element.9.refs_1_, f32[8,8,128]{2,1,0:T(8,128)S(1)} %get-tuple-element.10.refs_2_, ...), custom_call_target="tpu_custom_call" | custom-call | tf_op jit(solution)/shard_map/pallas_call | solution.py:801

commit v5 on v4

--- a/solution.py
+++ b/solution.py
@@ -483,7 +483,7 @@
             )
         return carry
 
-    lax.fori_loop(0, sequences // 2, update, 0)
+    lax.fori_loop(0, sequences // 4, update, 0)
     around(range(2, CUBE, 2), forward_mix, False)
     drain(gated_buf, recv_sems.at[1])
     drain(mix_buf.at[:, 1 - core], recv_sems.at[4])
@@ -498,7 +498,7 @@
     )
     pltpu.make_async_copy(columns_buf.at[plane], mixed_buf.at[plane], recv_sems.at[2]).start()
     line(lambda peer: columns_buf.at[peer], mixed_buf, 2)
-    lax.fori_loop(sequences // 2, sequences, update, 0)
+    lax.fori_loop(sequences // 4, sequences, update, 0)
     drain(mixed_buf, recv_sems.at[2])
     mixed = jnp.concatenate([mixed_buf[group] for group in range(groups)], axis=1)
     after_mix = (residual + rms_scale(mixed.astype(jnp.float32), postmix_ref[...])).astype(

time: 53.3 us -> 53.5 us (level)
  no operation moved by 1% of the time
where the time goes in v5:
time: 53.5 us; the launch traced here: 53.3 us
  Pallas kernels  52.7 us (99%)
  between operations  0.65 us (1%)
    pallas_call x1, Pallas kernels, layer(): pl.pallas_call(functools.partial(layer_kernel, n, groups), out_shape=(plt...  50.6 us
    pallas_call x1, Pallas kernels, publish(): pl.pallas_call(publish_kernel, out_shape=tuple((jax.ShapeDtypeStruct(r.sh...  2.07 us

profile of v5, /device:TPU:0, one launch (start us, length us, event | category | flops | bytes accessed | tf_op | source)
XLA Modules:
  0.0 53.3 jit_solution(10128671335514512577)
XLA Ops:
  0.6 50.6 %shard_map.264 = (bf16[8,2048]{1,0:T(8,128)(2,1)S(1)}, f32[8,8,128,128]{3,2,1,0:T(8,128)S(1)}, f32[8,8,128]{2,1,0:T(8,128)S(1)}, f32[8,8]{1,0:T(8,128)S(1)}) custom-call(bf16[8,2048]{1,0:T(8,128)(2,1)} %refs_0_.1, f32[1,2048]{1,0:T(1,128)} %bitcast.12, f32[1,2048]{1,0:T(1,128)} %bitcast.13, f32[1,2048]{1,0:T(1,128)} %bitcast.14, f32[1,2048]{1,0:T(1,128)} %bitcast.15, ...), custom_call_target="tpu_custom_call" | custom-call | tf_op jit(solution)/shard_map/pallas_call | solution.py:719
  51.3 2.1 %shard_map.265 = (bf16[8,2048]{1,0:T(8,128)(2,1)}, f32[8,8,128,128]{3,2,1,0:T(8,128)}, f32[8,8,128]{2,1,0:T(8,128)}, f32[8,8]{1,0:T(8,128)}) custom-call(bf16[8,2048]{1,0:T(8,128)(2,1)S(1)} %get-tuple-element.8.refs_0_, f32[8,8,128,128]{3,2,1,0:T(8,128)S(1)} %get-tuple-element.9.refs_1_, f32[8,8,128]{2,1,0:T(8,128)S(1)} %get-tuple-element.10.refs_2_, ...), custom_call_target="tpu_custom_call" | custom-call | tf_op jit(solution)/shard_map/pallas_call | solution.py:801
